TPU v7x, 512 devices: a whole 4x8x8 slice. The times are simulated.
512 devices in a mesh: dp: 4 (over x), kv: 64 (over z, y), tp: 2 (over core).
Axes of the slice: x: 4, y: 8, z: 8, core: 2. Of those that a mesh axis runs over, the one named last changes fastest.
Arguments:
- tokens: bfloat16 [4, 24576, 2048], P('dp', 'kv'), may hold values from -21 to 21
- seq_lengths: int32 [4], P('dp'), may hold values from 1 to 24576, 36864 in all
- block_picks: int32 [4, 384, 4, 16], P('dp', 'kv', 'tp'), may hold values from -1 to 377, as said below
- w_query: bfloat16 [2048, 1024], P('kv', 'tp'), may hold values from -0.125 to 0.125
- w_key: bfloat16 [2048, 256], P('kv', 'tp'), may hold values from -0.125 to 0.125
- w_value: bfloat16 [2048, 256], P('kv', 'tp'), may hold values from -0.125 to 0.125
- w_gate: bfloat16 [2048, 32], replicated, may hold values from -0.125 to 0.125
- w_ckey: bfloat16 [4096, 64], replicated, may hold values from -0.09375 to 0.09375
- w_cvalue: bfloat16 [4096, 64], replicated, may hold values from -0.09375 to 0.09375
- w_out: bfloat16 [1024, 2048], P('tp', 'kv'), may hold values from -0.1875 to 0.1875
Outputs:
- attention_out: bfloat16 [4, 24576, 2048], P('dp', ('kv', 'tp'))
Inputs may be any that keep to these rules, and one draw needn't show every extreme that they name: `block_picks`: A query block's entries name distinct blocks that all lie in earlier spans of 384 positions, or are -1; the largest such block is named in every draw. For one span and one group, the entries of all its query blocks together name blocks of any one other span at most 2 times; this is reached in every draw.
All inputs are finite; a program needn't handle non-finite values. No bound on the sum of `seq_lengths` on one device may be relied on, other than what follows from the above.
Results may differ from a plain program's by a relative error of at most 0.01.
The roundings to bfloat16 on the way count: a program that leaves them out, or rounds other values in their place, can miss the bound.
Values may be sent and summed in bfloat16 or wider, within the bound.
A program may use at most 64 MiB of HBM per device.

v0:
```python
import jax
import jax.numpy as jnp
from jax import lax
from jax.sharding import PartitionSpec as P

HEADS = 16
HEAD = 64
BLK = 64
PICKS = 16
CAP = 2


masked_low = -1e30


def in_one_piece(arrays, axis, dim, along):
    ends, at = ([], 0)
    for a in arrays[:-1]:
        at += a.shape[along]
        ends.append(at)
    both = jnp.concatenate(arrays, axis=along)
    return tuple(jnp.split(lax.all_gather(both, axis, axis=dim, tiled=True), ends, axis=along))


def sent_to_all(shard, axis):
    length = lax.axis_size(axis)
    return lax.all_to_all(
        jnp.broadcast_to(shard[None], (length, *shard.shape)), axis, 0, 0, tiled=True
    )


def in_order(pieces, dim):
    pieces = jnp.moveaxis(pieces, 0, dim)
    dims = pieces.shape
    return pieces.reshape(*dims[:dim], dims[dim] * dims[dim + 1], *dims[dim + 2 :])


def gathered_copies(shard, axis, dim):
    pieces = sent_to_all(shard, axis)
    return in_order(pieces, dim)


def split_up(shard, dim, length):
    dims = shard.shape
    pieces = shard.reshape(*dims[:dim], length, dims[dim] // length, *dims[dim + 1 :])
    return jnp.moveaxis(pieces, dim, 0)


def sum_at_owner(shard, axis, dim):
    pieces = split_up(shard, dim, lax.axis_size(axis))
    arrived = lax.all_to_all(pieces, axis, split_axis=0, concat_axis=0, tiled=True)
    return arrived.astype(jnp.float32).sum(axis=0)


def body(
    tokens, seq_lengths, block_picks, w_query, w_key, w_value, w_gate, w_ckey, w_cvalue, w_out
):
    token_rows = tokens[0]
    tok_count = token_rows.shape[0]
    shard_count = lax.axis_size("kv")
    shard_index = lax.axis_index("kv")
    head_index = lax.axis_index("tp")
    group_count = w_key.shape[1] // HEAD
    head_count = w_query.shape[1] // HEAD
    per_group = head_count // group_count
    block_count = tok_count // BLK
    inv_scale = HEAD ** (-0.5)
    zero_query = jnp.zeros((tok_count, w_query.shape[1]), jnp.float32)
    zero_key = jnp.zeros((tok_count, w_key.shape[1]), jnp.float32)
    runnings = (zero_query, zero_key, zero_key)
    weight_pieces = in_one_piece((w_query, w_key, w_value), "kv", 0, 1)
    collected = []
    for running, weight_piece in zip(runnings, weight_pieces):
        collected.append(jnp.dot(token_rows, weight_piece, preferred_element_type=jnp.float32))
    query_sum, key_sum, value_sum = tuple(collected)
    queries = query_sum.astype(jnp.bfloat16).reshape(block_count, BLK, group_count, per_group, HEAD)
    key_blocks = (
        key_sum.astype(jnp.bfloat16)
        .reshape(block_count, BLK, group_count, HEAD)
        .transpose(0, 2, 1, 3)
    )
    value_blocks = (
        value_sum.astype(jnp.bfloat16)
        .reshape(block_count, BLK, group_count, HEAD)
        .transpose(0, 2, 1, 3)
    )
    gate_all = jax.nn.sigmoid(jnp.dot(token_rows, w_gate, preferred_element_type=jnp.float32))
    gate_local = lax.dynamic_slice_in_dim(
        gate_all.reshape(tok_count, 2, HEADS), head_index * head_count, head_count, 2
    )
    gate_local = gate_local.reshape(block_count, BLK, 2, group_count, per_group)
    ckeys = jnp.dot(
        key_blocks.reshape(block_count * group_count, BLK * HEAD),
        w_ckey,
        preferred_element_type=jnp.float32,
    ).astype(jnp.bfloat16)
    cvalues = jnp.dot(
        value_blocks.reshape(block_count * group_count, BLK * HEAD),
        w_cvalue,
        preferred_element_type=jnp.float32,
    ).astype(jnp.bfloat16)
    cpairs = jnp.concatenate([ckeys, cvalues], axis=-1).reshape(block_count, group_count, 2 * HEAD)
    pair_blocks = jnp.concatenate([key_blocks, value_blocks], axis=-1)
    chosen = block_picks[0]
    usable = chosen >= 0
    group_ids = jnp.arange(group_count, dtype=jnp.int32)
    every_cpair = gathered_copies(cpairs, "kv", 0)
    owner_shard = jnp.where(usable, chosen // block_count, shard_count)
    within = jnp.where(usable, chosen % block_count, 0)
    listed = owner_shard.transpose(1, 0, 2).reshape(group_count, block_count * PICKS)
    owner_marks = (
        listed[:, :, None] == jnp.arange(shard_count, dtype=jnp.int32)[None, None, :]
    ).astype(jnp.int32)
    before = jnp.cumsum(owner_marks, axis=1) - owner_marks
    slot_rank = jnp.sum(before * owner_marks, axis=2)
    slot_rank = slot_rank.reshape(group_count, block_count, PICKS).transpose(1, 0, 2)
    slot_index = group_ids[None, :, None] * CAP + slot_rank
    request = jnp.zeros((shard_count, group_count * CAP), jnp.int32)
    request = request.at[owner_shard, slot_index].set(within, mode="drop")
    asked_blocks = lax.all_to_all(request, "kv", split_axis=0, concat_axis=0, tiled=True)
    slot_group = jnp.arange(group_count * CAP, dtype=jnp.int32) // CAP
    reply_blocks = pair_blocks[asked_blocks, slot_group[None, :]]
    returned = lax.all_to_all(reply_blocks, "kv", split_axis=0, concat_axis=0, tiled=True)
    flat_pairs = returned.reshape(-1, BLK, 2 * HEAD)
    lookup = jnp.where(usable, owner_shard * (group_count * CAP) + slot_index, 0)
    fetched = flat_pairs[lookup]
    comp_keys = every_cpair[..., :HEAD]
    comp_values = every_cpair[..., HEAD:]
    block_ends = jnp.arange(every_cpair.shape[0], dtype=jnp.int32) * BLK + (BLK - 1)
    causal = jnp.arange(BLK)[None, :] <= jnp.arange(BLK)[:, None]

    def attend(block_inputs):
        qblock, gblock, own_pair, far_pair, far_usable, block_index = block_inputs
        query_spots = shard_index * tok_count + block_index * BLK + jnp.arange(BLK, dtype=jnp.int32)
        comp_score = (
            jnp.einsum("tgpd,cgd->gtpc", qblock, comp_keys, preferred_element_type=jnp.float32)
            * inv_scale
        )
        visible = (block_ends[None, :] <= query_spots[:, None])[None, :, None, :]
        comp_score = jnp.where(visible, comp_score, masked_low)
        comp_top = jnp.max(comp_score, axis=-1, keepdims=True)
        comp_weight = jnp.where(visible, jnp.exp(comp_score - comp_top), 0.0)
        comp_sum = jnp.maximum(jnp.sum(comp_weight, axis=-1, keepdims=True), 1.0)
        comp_prob = (comp_weight / comp_sum).astype(jnp.bfloat16)
        comp_out = jnp.einsum(
            "gtpc,cgd->tgpd", comp_prob, comp_values, preferred_element_type=jnp.float32
        )
        far_pairs = far_pair.reshape(group_count, PICKS * BLK, 2 * HEAD)
        own_score = (
            jnp.einsum(
                "tgpd,gsd->gtps", qblock, own_pair[..., :HEAD], preferred_element_type=jnp.float32
            )
            * inv_scale
        )
        own_mask = causal[None, :, None, :]
        own_score = jnp.where(own_mask, own_score, masked_low)
        far_score = (
            jnp.einsum(
                "tgpd,gkd->gtpk", qblock, far_pairs[..., :HEAD], preferred_element_type=jnp.float32
            )
            * inv_scale
        )
        far_mask = jnp.repeat(far_usable, BLK, axis=-1)[:, None, None, :]
        far_score = jnp.where(far_mask, far_score, masked_low)
        score_top = jnp.maximum(
            jnp.max(own_score, axis=-1, keepdims=True), jnp.max(far_score, axis=-1, keepdims=True)
        )
        own_weight = jnp.where(own_mask, jnp.exp(own_score - score_top), 0.0)
        far_weight = jnp.where(far_mask, jnp.exp(far_score - score_top), 0.0)
        normalizer = jnp.sum(own_weight, axis=-1, keepdims=True) + jnp.sum(
            far_weight, axis=-1, keepdims=True
        )
        own_prob = (own_weight / normalizer).astype(jnp.bfloat16)
        far_prob = (far_weight / normalizer).astype(jnp.bfloat16)
        chosen_out = jnp.einsum(
            "gtps,gsd->tgpd", own_prob, own_pair[..., HEAD:], preferred_element_type=jnp.float32
        ) + jnp.einsum(
            "gtpk,gkd->tgpd", far_prob, far_pairs[..., HEAD:], preferred_element_type=jnp.float32
        )
        mixed_out = gblock[:, 0, :, :, None] * comp_out + gblock[:, 1, :, :, None] * chosen_out
        return mixed_out.astype(jnp.bfloat16)

    attended = lax.map(
        attend,
        (
            queries,
            gate_local,
            pair_blocks,
            fetched,
            usable,
            jnp.arange(block_count, dtype=jnp.int32),
        ),
    )
    attended = attended.reshape(tok_count, head_count * HEAD)
    out_full = lax.all_gather(w_out, "kv", axis=1, tiled=True)
    half_rows = tok_count // lax.axis_size("tp")
    summed = sum_at_owner(
        jnp.dot(attended, out_full, preferred_element_type=jnp.float32).astype(jnp.bfloat16),
        "tp",
        0,
    )
    out_positions = (
        shard_index * tok_count + head_index * half_rows + jnp.arange(half_rows, dtype=jnp.int32)
    )
    live_rows = out_positions < seq_lengths[0]
    return jnp.where(live_rows[:, None], summed, 0.0).astype(jnp.bfloat16)[None]


def solution(mesh):
    return jax.shard_map(
        body,
        mesh=mesh,
        in_specs=(
            P("dp", "kv", None),
            P("dp"),
            P("dp", "kv", "tp", None),
            P("kv", "tp"),
            P("kv", "tp"),
            P("kv", "tp"),
            P(),
            P(),
            P(),
            P("tp", "kv"),
        ),
        out_specs=P("dp", ("kv", "tp"), None),
        check_vma=False,
    )
```

profile of v0, /device:TPU:87, one launch (start us, length us, event | category | flops | bytes accessed | tf_op | source)
XLA Modules:
  0.0 315.6 jit_solution(17782680792332563680)
XLA Ops:
  6.5 1.5 pad_maximum_fusion.1
  11.2 9.4 %scatter_fusion = s32[64,4]{0,1:T(4,128)S(1)} fusion(s32[64,4]{0,1:T(4,128)S(1)} %broadcast.259, s32[192]{0:T(256)S(1)} %reshape.293, s32[192]{0:T(256)S(1)} %reshape.295), kind=kCustom, calls=%fused_computation.2 | custom fusion | bytes 3840 | tf_op jit(solution)/shard_map/scatter | solution.py:119
  21.3 15.0 %all-to-all-start.1 = ((s32[64,1,4]{2,1,0:T(1,128)}), s32[64,1,4]{2,1,0:T(1,128)S(1)}, u32[]{:S(2)}, u32[]{:S(2)}) async-start(s32[64,1,4]{2,1,0:T(1,128)} %copy.82), calls=%async_computation.1 | async-start | bytes 65536 | tf_op jit(solution)/shard_map/all_to_all | solution.py:120
  36.3 57.7 %all-gather.3.cloned.1.call-done = bf16[2048,768]{1,0:T(8,128)(2,1)} async-done(((bf16[32,768]{1,0:T(8,128)(2,1)}), bf16[2048,768]{1,0:T(8,128)(2,1)}) %all-gather.3.cloned.1.call-update) | async-done | bytes 3145744 | tf_op jit(solution)/shard_map/all_gather | solution.py:22
  94.0 1.6 fusion.77
  96.2 1.6 fusion.80
  99.9 9.1 %all-to-all-start = ((bf16[64,6,2,128]{3,2,1,0:T(2,128)(2,1)}), bf16[64,6,2,128]{3,2,1,0:T(2,128)(2,1)S(1)}, u32[]{:S(2)}, u32[]{:S(2)}) async-start(bf16[64,6,2,128]{3,2,1,0:T(2,128)(2,1)} %broadcast_in_dim.153), calls=%async_computation | async-start | bytes 393216 | tf_op jit(solution)/shard_map/all_to_all | solution.py:27
  109.3 3.4 %gather_fusion = bf16[256,64,128]{2,1,0:T(8,128)(2,1)} fusion(bf16[6,2,64,128]{3,2,1,0:T(8,128)(2,1)S(1)} %pad_maximum_fusion, s32[256]{0:T(256)S(1)} %reshape.279), kind=kCustom, calls=%fused_computation | custom fusion | bytes 8390656 | tf_op jit(solution)/shard_map/gather | solution.py:122
  112.7 6.4 %all-to-all-done = bf16[64,6,2,128]{3,2,1,0:T(2,128)(2,1)S(1)} async-done(((bf16[64,6,2,128]{3,2,1,0:T(2,128)(2,1)}), bf16[64,6,2,128]{3,2,1,0:T(2,128)(2,1)S(1)}, u32[]{:S(2)}, u32[]{:S(2)}) %all-to-all-start) | async-done | bytes 196640 | tf_op jit(solution)/shard_map/all_to_all | solution.py:27
  119.0 7.7 %all-to-all-start.2 = ((bf16[64,4,64,128]{3,2,1,0:T(8,128)(2,1)}), bf16[64,4,64,128]{3,2,1,0:T(8,128)(2,1)}, u32[]{:S(2)}, u32[]{:S(2)}) async-start(bf16[64,4,64,128]{3,2,1,0:T(8,128)(2,1)} %bitcast.270), calls=%async_computation.2 | async-start | bytes 8388608 | tf_op jit(solution)/shard_map/all_to_all | solution.py:123
  129.0 2.9 fusion.66
  131.9 1.6 reshape.308
  133.5 1.7 copy.85
  135.9 96.3 %all-to-all-done.2 = bf16[64,4,64,128]{3,2,1,0:T(8,128)(2,1)} async-done(((bf16[64,4,64,128]{3,2,1,0:T(8,128)(2,1)}), bf16[64,4,64,128]{3,2,1,0:T(8,128)(2,1)}, u32[]{:S(2)}, u32[]{:S(2)}) %all-to-all-start.2) | async-done | bytes 4194336 | tf_op jit(solution)/shard_map/all_to_all | solution.py:123
  232.2 4.9 %gather_fusion.1 = bf16[192,64,128]{2,1,0:T(8,128)(2,1)} fusion(bf16[256,64,128]{2,1,0:T(8,128)(2,1)} %bitcast.22, s32[1024]{0:T(1024)S(1)} %pad_clamp_fusion), kind=kCustom, calls=%fused_computation.1 | custom fusion | bytes 6292224 | tf_op jit(solution)/shard_map/gather | solution.py:126
  237.1 54.6 %while.14 = (s32[]{:T(128)}, bf16[6,64,2,4,64]{4,3,2,1,0:T(4,128)(2,1)}, f32[6,64,2,2,4]{1,0,4,3,2:T(8,128)S(1)}, s32[6]{0:T(128)S(1)}, s32[]{:T(128)}, /*index=...) while((s32[]{:T(128)}, ...), condition=%wide.region_10.11_spmd.clone.clone, body=%wide.region_3.10_spmd.clone.clone.sunk | while | flops 202175168 | bytes 12035885 | solution.py:183
  242.7 1.3 fusion.155
  244.0 1.5 fusion.156
  251.8 1.3 fusion.155
  253.1 1.5 fusion.156
  260.9 1.3 fusion.155
  262.2 1.5 fusion.156
  270.0 1.3 fusion.155
  271.3 1.5 fusion.156
  279.1 1.3 fusion.155
  280.4 1.5 fusion.156
  288.2 1.3 fusion.155
  289.5 1.5 fusion.156
  291.7 2.0 reshape.276
  293.8 2.6 convolution_convert_fusion
  296.4 11.0 %all_to_all.27 = bf16[2,192,2048]{2,1,0:T(8,128)(2,1)S(1)} all-to-all(bf16[2,192,2048]{2,1,0:T(8,128)(2,1)S(1)} %bitcast.277), channel_id=1, replica_groups=mesh['dp'=4,'kv'=64,'tp'=2] {'tp'}, dimensions={0} | all-to-all | bytes 3145728 | tf_op jit(solution)/shard_map/all_to_all | solution.py:51
  307.7 1.1 fusion.53
  (193 shorter events, 42.5 us)
Async XLA Ops:
  6.5 87.4 %copy-start = (bf16[1,384,2048]{2,1,0:T(8,128)(2,1)S(1)}, bf16[1,384,2048]{2,1,0:T(8,128)(2,1)}, u32[]{:S(2)}) copy-start(bf16[1,384,2048]{2,1,0:T(8,128)(2,1)} %param.12) | copy-start | bytes 4718596
  6.5 87.4 %all-gather.3.cloned.1.call-start = ((), (), s32[]{:S(2)}) async-start(), calls=%async_computation.4 | async-start | bytes 3194880 | tf_op jit(solution)/shard_map/all_gather | solution.py:22
  21.3 77.8 %all-to-all-start.1 = ((s32[64,1,4]{2,1,0:T(1,128)}), s32[64,1,4]{2,1,0:T(1,128)S(1)}, u32[]{:S(2)}, u32[]{:S(2)}) async-start(s32[64,1,4]{2,1,0:T(1,128)} %copy.82), calls=%async_computation.1 | async-start | bytes 65536 | tf_op jit(solution)/shard_map/all_to_all | solution.py:120
  95.8 2.7 copy-start.1
  96.0 2.7 copy-start.2
  99.9 19.1 %all-to-all-start = ((bf16[64,6,2,128]{3,2,1,0:T(2,128)(2,1)}), bf16[64,6,2,128]{3,2,1,0:T(2,128)(2,1)S(1)}, u32[]{:S(2)}, u32[]{:S(2)}) async-start(bf16[64,6,2,128]{3,2,1,0:T(2,128)(2,1)} %broadcast_in_dim.153), calls=%async_computation | async-start | bytes 393216 | tf_op jit(solution)/shard_map/all_to_all | solution.py:27
  119.0 8.4 %copy-start.3 = (bf16[2048,32]{0,1:T(8,128)(2,1)S(1)}, bf16[2048,32]{0,1:T(8,128)(2,1)}, u32[]{:S(2)}) copy-start(bf16[2048,32]{0,1:T(8,128)(2,1)} %param.18) | copy-start | bytes 393220
  119.0 9.1 %copy-start.4 = (s32[1,6,2,16]{3,2,1,0:T(2,128)S(1)}, s32[1,6,2,16]{3,2,1,0:T(2,128)}, u32[]{:S(2)}) copy-start(s32[1,6,2,16]{3,2,1,0:T(2,128)} %param.14) | copy-start | bytes 2308
  119.0 113.2 %all-to-all-start.2 = ((bf16[64,4,64,128]{3,2,1,0:T(8,128)(2,1)}), bf16[64,4,64,128]{3,2,1,0:T(8,128)(2,1)}, u32[]{:S(2)}, u32[]{:S(2)}) async-start(bf16[64,4,64,128]{3,2,1,0:T(8,128)(2,1)} %bitcast.270), calls=%async_computation.2 | async-start | bytes 8388608 | tf_op jit(solution)/shard_map/all_to_all | solution.py:123
  126.7 167.1 %all-gather.5.cloned.1.call-start = ((), (), s32[]{:S(2)}) async-start(), calls=%async_computation.5 | async-start | bytes 2129920 | tf_op jit(solution)/shard_map/all_gather | solution.py:195
Sparse Core Ops, SparseCore 0:
  10.3 83.5 all-gather.2
  130.6 149.2 all-gather.4
where the time goes:
time: 317 us; the launch traced here: 316 us
  waiting for transfers between devices  161 us (51%)
  local copies, waits for them, and re-layouts  43.3 us (14%)
  matrix products  38.5 us (12%)
  starting transfers between devices  32 us (10%)
  between operations  14.4 us (5%)
  blocking collectives  11 us (3%)
  other arithmetic  10.8 us (3%)
  loops' own time  4.77 us (2%)
    all_to_all x1, waiting for transfers between devices, body(): lax.all_to_all(reply_blocks, 'kv', split_axis=0, concat_axis=0, tiled=True)  96.3 us
    all_gather x1, waiting for transfers between devices, in_one_piece(): lax.all_gather(both, axis, axis=dim, tiled=True)  57.7 us
    all_to_all x1, starting transfers between devices, body(): lax.all_to_all(request, 'kv', split_axis=0, concat_axis=0, tiled=True)  15 us
    all_to_all x1, blocking collectives, sum_at_owner(): lax.all_to_all(pieces, axis, split_axis=0, concat_axis=0, tiled=True)  11 us
    dynamic_slice x18, local copies, waits for them, and re-layouts, body(): lax.map(attend, (queries, gate_local, pair_blocks, fetched, usable, jnp.a...  10.6 us
    scatter x1, local copies, waits for them, and re-layouts, body(): request = request.at[owner_shard, slot_index].set(within, mode='drop')  9.44 us
    all_to_all x1, starting transfers between devices, sent_to_all(): lax.all_to_all(jnp.broadcast_to(shard[None], (length, *shard.shape)), axi...  9.13 us
    dot_general x6, matrix products, attend(): jnp.einsum('gtpc,cgd->tgpd', comp_prob, comp_values, preferred_element_ty...  8.76 us
  transfers between devices with their start and end apart: 5, of which 3 were waited for; matrix products, arithmetic and copies ran while one was open for 27% of the time, Pallas kernels for 0%

commit v1 on v0

v1 whole, which is shorter than its diff:
```python
import functools

import jax
import jax.numpy as jnp
from jax import lax
from jax.experimental import pallas as pl
from jax.experimental.pallas import tpu as pltpu
from jax.sharding import PartitionSpec as P

MESH = pl.DeviceIdType.MESH

HEADS = 16
GROUPS = 4
PER = 4
HEAD = 64
BLK = 64
PICKS = 16
N = 8
ROWS = 208
HALF = 192
SPLIT = 112
MASKED = -1e30
VMEM = pltpu.MemorySpace.VMEM
SMEM = pltpu.MemorySpace.SMEM
HBM = pltpu.MemorySpace.HBM


def place():
    kv = lax.axis_index("kv")
    return kv // N, lax.rem(kv, N)


class Copies:
    def __init__(self, send_sems, recv_sems):
        self.send_sems, self.recv_sems, self.used, self.sent = send_sems, recv_sems, 0, []

    def slot(self):
        self.used += 1
        return self.used - 1

    def send(self, i, src, dst, device):
        copy = pltpu.make_async_remote_copy(
            src_ref=src,
            dst_ref=dst,
            send_sem=self.send_sems.at[i],
            recv_sem=self.recv_sems.at[i],
            device_id=device,
            device_id_type=MESH,
        )
        copy.start()

    def arrived(self, i, ref, device):
        pltpu.make_async_remote_copy(
            src_ref=ref,
            dst_ref=ref,
            send_sem=self.send_sems.at[i],
            recv_sem=self.recv_sems.at[i],
            device_id=device,
            device_id_type=MESH,
        ).wait_recv()

    def left(self, i, ref, device):
        pltpu.make_async_remote_copy(
            src_ref=ref,
            dst_ref=ref,
            send_sem=self.send_sems.at[i],
            recv_sem=self.recv_sems.at[i],
            device_id=device,
            device_id_type=MESH,
        ).wait_send()


def when(cond, fn):
    if cond is True:
        fn()
    elif cond is not False:
        pl.when(cond)(fn)


def both(a, b):
    if a is True:
        return b
    if b is True:
        return a
    if a is False or b is False:
        return False
    return jnp.logical_and(a, b)


def wrap(i):
    return lax.rem(i + N, N)


def barrier(kinds):
    sem = pltpu.get_barrier_semaphore()
    for device in kinds:
        pl.semaphore_signal(sem, inc=1, device_id=device, device_id_type=MESH)
    pl.semaphore_wait(sem, len(kinds))


def plane_partners(z, y):
    return [{"kv": z * N + wrap(y + d)} for d in range(1, N)] + [
        {"kv": wrap(z + d) * N + y} for d in range(1, N)
    ]


class Gather:
    def __init__(self, copies, src, view, rows, causal, pair):
        self.c, self.src, self.view, self.rows, self.causal, self.pair = (
            copies,
            src,
            view,
            rows,
            causal,
            pair,
        )
        self.z, self.y = place()
        self.live = True if rows == N else self.z < rows
        self.waits = []
        self.pair_waits = []
        self.pending = []

    def dev(self, z, y):
        return {"kv": z * N + y}

    def transfer(self, cond_send, src, dst, device, cond_recv, got):
        i = self.c.slot()
        when(cond_send, lambda: self.c.send(i, src, dst, device))
        self.waits.append((i, cond_send, src, device))
        return (i, cond_recv, got, device)

    def take(self, t):
        i, cond, ref, device = t
        when(cond, lambda: self.c.arrived(i, ref, device))

    def mirror(self, cond, ref):
        if self.pair is None:
            return
        i = self.c.slot()
        when(cond, lambda: self.c.send(i, ref, ref, self.pair))
        self.pair_waits.append((i, cond, ref))

    def first(self):
        z, y = self.z, self.y
        self.a1, self.b1 = [], []
        for d in range(1, N):
            self.a1.append(
                self.transfer(
                    self.live,
                    self.src(0),
                    self.view(z, 1, y, 1, 0),
                    self.dev(z, wrap(y + d)),
                    self.live,
                    self.view(z, 1, wrap(y - d), 1, 0),
                )
            )
        for d in range(1, N) if not self.causal else range(1, self.rows):
            cs = True if not self.causal else z + d < self.rows
            cr = True if not self.causal else both(self.live, z - d >= 0)
            self.b1.append(
                self.transfer(
                    cs,
                    self.src(1),
                    self.view(z, 1, y, 1, 1),
                    self.dev(wrap(z + d), y),
                    cr,
                    self.view(wrap(z - d), 1, y, 1, 1),
                )
            )

    def hop_a(self, right, sub, k, depth):
        z, y = self.z, self.y
        y0, ny = (sub * 4, 4)
        if right:
            o, got, to = wrap(z - (k - 1)), wrap(z - k), wrap(z + 1)
            cs = both(z - (k - 1) >= 0, z + 1 < self.rows) if self.causal else True
            cr = both(self.live, z - k >= 0) if self.causal else True
        else:
            o, got, to = wrap(z + k - 1), lax.rem(z + k, N), wrap(z - 1)
            cs = o < depth if self.causal else True
            cr = got < depth if self.causal else True
        return self.transfer(
            cs,
            self.view(o, 1, y0, ny, 0),
            self.view(o, 1, y0, ny, 0),
            self.dev(to, y),
            cr,
            self.view(got, 1, y0, ny, 0),
        )

    def hop_b(self, right, sub, k):
        z, y = self.z, self.y
        if self.rows == N:
            z0, nz = sub * 4, 4
            cond = True if (sub == 0 or not self.causal) else z >= 4
        else:
            z0, nz = 0, self.rows
            cond = self.live
        if right:
            o, got, to = wrap(y - (k - 1)), wrap(y - k), wrap(y + 1)
        else:
            o, got, to = lax.rem(y + k - 1, N), lax.rem(y + k, N), wrap(y - 1)
        return self.transfer(
            cond,
            self.view(z0, nz, o, 1, 1),
            self.view(z0, nz, o, 1, 1),
            self.dev(z, to),
            cond,
            self.view(z0, nz, got, 1, 1),
        )

    def depth_a(self, right, sub):
        if self.rows < N:
            return self.rows - 1 if right else 0
        return 4 if right == (sub == 0) else 3

    def depth_b(self, right, sub):
        if self.rows < N and sub == 1:
            return 0
        return 4 if right == (sub == 0) else 3

    def lanes(self):
        return [(r, s) for s in (0, 1) for r in (True, False)]

    def hop(self, k):
        if k == 1:
            self.flight = {}
        for ring in ("a", "b"):
            if k == 1:
                for t in self.a1 if ring == "a" else self.b1:
                    self.take(t)
            for r, s in self.lanes():
                depth = self.depth_a(r, s) if ring == "a" else self.depth_b(r, s)
                if k > 1 and k - 1 <= depth:
                    t = self.flight[ring, r, s]
                    self.take(t)
                    self.pending.append((t[1], t[2]))
                if k <= depth:
                    self.flight[ring, r, s] = (
                        self.hop_a(r, s, k, depth) if ring == "a" else self.hop_b(r, s, k)
                    )
            if k == 1:
                if ring == "a":
                    self.pending.append((self.live, self.view(self.z, 1, 0, N, 0)))
                else:
                    self.pending.append(
                        (self.live, self.view(0, N if self.rows == N else self.rows, self.y, 1, 1))
                    )
        for cond, ref in self.pending:
            self.mirror(cond, ref)
        self.pending = []

    def last(self):
        for i, cond, ref in self.pair_waits:
            when(cond, lambda: self.c.arrived(i, ref, self.pair))
            when(cond, lambda: self.c.left(i, ref, self.pair))
        for i, cond, ref, device in self.waits:
            when(cond, lambda: self.c.left(i, ref, device))


def weights_kernel(src_ref, out_ref, send_sems, recv_sems):
    z, y = place()
    rows, cols = src_ref.shape
    half = cols // 2
    barrier(plane_partners(z, y))
    out_ref[z, y] = src_ref[...]
    c = Copies(send_sems, recv_sems)

    def src(part):
        return src_ref.at[:, pl.ds(part * half, half)]

    def view(z0, nz, y0, ny, part):
        zi = z0 if nz == 1 else pl.ds(z0, nz)
        yi = y0 if ny == 1 else pl.ds(y0, ny)
        return out_ref.at[zi, yi, :, pl.ds(part * half, half)]

    g = Gather(c, src, view, N, False, None)
    g.first()
    for k in range(1, 6):
        g.hop(k)
    g.last()


def gather_weights(piece):
    rows, cols = piece.shape
    return pl.pallas_call(
        weights_kernel,
        out_shape=jax.ShapeDtypeStruct((N, N, rows, cols), piece.dtype),
        in_specs=[pl.BlockSpec(memory_space=VMEM)],
        out_specs=pl.BlockSpec(memory_space=VMEM),
        scratch_shapes=[pltpu.SemaphoreType.DMA((64,)), pltpu.SemaphoreType.DMA((64,))],
        compiler_params=pltpu.CompilerParams(
            collective_id=0, has_side_effects=True, vmem_limit_bytes=24 << 20
        ),
        name="gather_weights",
    )(piece)


def spread_kernel(main_ref, ints_ref, got_ref, gint_ref, send_sems, recv_sems):
    dp, tp = lax.axis_index("dp"), lax.axis_index("tp")
    others = []
    for e in range(1, 8):
        d, t = e // 2, e % 2
        others.append({"dp": lax.rem(dp + d, 4), "tp": lax.rem(tp + t, 2)})
    barrier(others)
    c = Copies(send_sems, recv_sems)
    mine = dp // 2 == tp
    for gl in range(2):
        for h in range(2):
            g = 2 * tp + gl
            own = jnp.logical_and(g == dp, tp == h)
            device = {"dp": g, "tp": jnp.int32(h)}
            i = (gl * 2 + h) * 2

            def go(gl=gl, h=h, device=device):
                for k, (s, d) in enumerate(((main_ref, got_ref), (ints_ref, gint_ref))):
                    pltpu.make_async_remote_copy(
                        src_ref=s.at[gl, h],
                        dst_ref=d.at[dp],
                        send_sem=send_sems.at[(gl * 2 + h) * 2 + k],
                        recv_sem=recv_sems.at[dp, k],
                        device_id=device,
                        device_id_type=MESH,
                    ).start()

            def keep(gl=gl, h=h):
                got_ref[dp] = main_ref[gl, h]
                gint_ref[dp] = ints_ref[gl, h]

            pl.when(jnp.logical_not(own))(go)
            pl.when(own)(keep)
    for q in range(4):
        theirs = jnp.logical_not(jnp.logical_and(q == dp, mine))

        def take(q=q):
            for k, d in enumerate((got_ref, gint_ref)):
                pltpu.make_async_remote_copy(
                    src_ref=d.at[q],
                    dst_ref=d.at[q],
                    send_sem=send_sems.at[k],
                    recv_sem=recv_sems.at[q, k],
                    device_id={"dp": jnp.int32(q), "tp": tp},
                    device_id_type=MESH,
                ).wait_recv()

        pl.when(theirs)(take)
    for gl in range(2):
        for h in range(2):
            g = 2 * tp + gl
            own = jnp.logical_and(g == dp, tp == h)

            def done(gl=gl, h=h, g=g):
                for k, s in enumerate((main_ref, ints_ref)):
                    pltpu.make_async_remote_copy(
                        src_ref=s.at[gl, h],
                        dst_ref=s.at[gl, h],
                        send_sem=send_sems.at[(gl * 2 + h) * 2 + k],
                        recv_sem=recv_sems.at[0, k],
                        device_id={"dp": g, "tp": jnp.int32(h)},
                        device_id_type=MESH,
                    ).wait_send()

            pl.when(jnp.logical_not(own))(done)


def spread(main, ints):
    return pl.pallas_call(
        spread_kernel,
        out_shape=[
            jax.ShapeDtypeStruct((4,) + main.shape[2:], main.dtype),
            jax.ShapeDtypeStruct((4,) + ints.shape[2:], ints.dtype),
        ],
        in_specs=[pl.BlockSpec(memory_space=VMEM)] * 2,
        out_specs=[pl.BlockSpec(memory_space=VMEM)] * 2,
        scratch_shapes=[pltpu.SemaphoreType.DMA((8,)), pltpu.SemaphoreType.DMA((4, 2))],
        compiler_params=pltpu.CompilerParams(
            collective_id=1, has_side_effects=True, vmem_limit_bytes=16 << 20
        ),
        name="spread",
    )(main, ints)


def kv_kernel(spans, src_ref, *refs):
    outs, (send_sems, recv_sems) = refs[: len(spans)], refs[len(spans) :]
    z, y = place()
    tp = lax.axis_index("tp")
    pair = {"tp": 1 - tp}
    barrier(plane_partners(z, y) + [pair])
    c = Copies(send_sems, recv_sems)
    jobs = []
    for r, rows in enumerate(spans):
        out_ref = outs[r]

        def own(out_ref=out_ref, r=r):
            out_ref[tp, z, y] = src_ref[r]

        when(True if rows == N else z < rows, own)

        def src(part, r=r):
            return src_ref.at[r, pl.ds(0, SPLIT) if part == 0 else pl.ds(SPLIT, ROWS - SPLIT)]

        def view(z0, nz, y0, ny, part, out_ref=out_ref):
            zi = z0 if nz == 1 else pl.ds(z0, nz)
            yi = y0 if ny == 1 else pl.ds(y0, ny)
            rows_of = pl.ds(0, SPLIT) if part == 0 else pl.ds(SPLIT, ROWS - SPLIT)
            return out_ref.at[tp, zi, yi, rows_of]

        jobs.append(Gather(c, src, view, rows, True, pair))
    for g in jobs:
        g.first()
    for k in range(1, 6):
        for g in jobs:
            g.hop(k)
    for g in jobs:
        g.last()


def gather_kv(src, spans, number):
    return pl.pallas_call(
        functools.partial(kv_kernel, spans),
        out_shape=[jax.ShapeDtypeStruct((2, rows, N, ROWS, 2 * HEAD), src.dtype) for rows in spans],
        in_specs=[pl.BlockSpec(memory_space=VMEM)],
        out_specs=[pl.BlockSpec(memory_space=VMEM)] * len(spans),
        scratch_shapes=[pltpu.SemaphoreType.DMA((320,)), pltpu.SemaphoreType.DMA((320,))],
        compiler_params=pltpu.CompilerParams(
            collective_id=number, has_side_effects=True, vmem_limit_bytes=40 << 20
        ),
        name="gather_kv",
    )(src)


def attend_kernel(spans, order_ref, lens_ref, picks_ref, main_ref, gate_ref, bias_ref, comp_ref, *refs):
    kv_refs, (out_ref, buf, sems) = refs[: len(spans)], refs[len(spans) :]
    kv, tp = lax.axis_index("kv"), lax.axis_index("tp")
    start = kv * (2 * HALF) + tp * HALF
    for r, rows in enumerate(spans):
        seq = order_ref[r]

        @pl.when(jnp.logical_and(start < lens_ref[seq], kv < rows * N))
        def _(r=r, seq=seq):
            def fetch(n, carry):
                j = n // PICKS
                p = lax.rem(n, PICKS)
                b = jnp.maximum(picks_ref[seq, j, p], 0)
                span = b // 6
                at = b - span * 6
                t = at // 3
                row = (at - t * 3) * BLK
                pltpu.make_async_copy(
                    kv_refs[r].at[t, span // N, lax.rem(span, N), pl.ds(pl.multiple_of(row, BLK), BLK)],
                    buf.at[r * 3 + j, pl.ds(pl.multiple_of(p * BLK, BLK), BLK)],
                    sems.at[r * 3 + j],
                ).start()
                return carry

            lax.fori_loop(0, 3 * PICKS, fetch, 0)

    lane = lax.broadcasted_iota(jnp.int32, (BLK, 128), 1)
    row_in = lax.rem(lax.broadcasted_iota(jnp.int32, (PER * BLK, 1), 0), BLK)

    def step(n, carry):
        r = n // 3
        j = n - r * 3
        seq = order_ref[r]
        rows = pl.ds(pl.multiple_of(j * BLK, BLK), BLK)
        live = start < lens_ref[seq]

        @pl.when(jnp.logical_not(live))
        def _():
            out_ref[seq, rows] = jnp.zeros((BLK, PER * HEAD), jnp.bfloat16)

        @pl.when(live)
        def _():
            pltpu.make_async_copy(buf.at[n], buf.at[n], sems.at[n]).wait()
            parts = []
            for h in range(PER):
                two = main_ref[seq, rows, pl.ds((h // 2) * 128, 128)].astype(jnp.float32) * 0.125
                if h % 2:
                    two = pltpu.roll(two, 64, 1)
                parts.append(jnp.where(lane < HEAD, two, 0.0).astype(jnp.bfloat16))
            q = jnp.concatenate(parts, axis=0)

            def score(keys):
                return lax.dot_general(
                    q, keys, (((1,), (1,)), ((), ())), preferred_element_type=jnp.float32
                )

            spot = start + j * BLK + row_in
            comp = comp_ref[r]
            ends = lax.broadcasted_iota(jnp.int32, (1, comp.shape[0]), 1) * BLK + (BLK - 1)
            seen = ends <= spot
            cs = jnp.where(seen, score(comp), MASKED)
            ctop = jnp.max(cs, axis=-1, keepdims=True)
            cw = jnp.where(seen, jnp.exp(cs - ctop), 0.0)
            cn = jnp.maximum(jnp.sum(cw, axis=-1, keepdims=True), 1.0)
            cp = (cw * (1.0 / cn)).astype(jnp.bfloat16)
            co = jnp.dot(cp, comp, preferred_element_type=jnp.float32)

            own = main_ref[seq, rows, pl.ds(PER * HEAD, 128)]
            far = buf[n]
            ks = lax.broadcasted_iota(jnp.int32, (1, BLK), 1)
            os = jnp.where(ks <= row_in, score(own), MASKED)
            fs = jnp.where(bias_ref[seq, j] > 0.5, score(far), MASKED)
            top = jnp.maximum(
                jnp.max(os, axis=-1, keepdims=True), jnp.max(fs, axis=-1, keepdims=True)
            )
            ow, fw = jnp.exp(os - top), jnp.exp(fs - top)
            inv = 1.0 / (jnp.sum(ow, axis=-1, keepdims=True) + jnp.sum(fw, axis=-1, keepdims=True))
            so = jnp.dot(
                (ow * inv).astype(jnp.bfloat16), own, preferred_element_type=jnp.float32
            ) + jnp.dot((fw * inv).astype(jnp.bfloat16), far, preferred_element_type=jnp.float32)
            mixed = []
            gates = gate_ref[seq, rows]
            for h in range(PER):
                at = slice(h * BLK, (h + 1) * BLK)
                mixed.append(gates[:, h : h + 1] * co[at] + gates[:, 4 + h : 5 + h] * so[at])
            for h in range(2):
                pair = jnp.where(lane < HEAD, pltpu.roll(mixed[2 * h], 64, 1), mixed[2 * h + 1])
                out_ref[seq, rows, pl.ds(h * 128, 128)] = pair.astype(jnp.bfloat16)

        return carry

    lax.fori_loop(0, 12, step, 0)


def attend(spans, order, lens, picks, main, gates, bias, comp, gathered):
    vm = pl.BlockSpec(memory_space=VMEM)
    sm = pl.BlockSpec(memory_space=SMEM)
    return pl.pallas_call(
        functools.partial(attend_kernel, spans),
        out_shape=jax.ShapeDtypeStruct((4, HALF, PER * HEAD), jnp.bfloat16),
        in_specs=[sm, sm, sm, vm, vm, vm, vm] + [pl.BlockSpec(memory_space=HBM)] * len(spans),
        out_specs=vm,
        scratch_shapes=[
            pltpu.VMEM((12, PICKS * BLK, 2 * HEAD), jnp.bfloat16),
            pltpu.SemaphoreType.DMA((12,)),
        ],
        compiler_params=pltpu.CompilerParams(vmem_limit_bytes=32 << 20),
        name="attend",
    )(order, lens, picks, main, gates, bias, comp, *gathered)


def by_halves(a):
    return a.reshape(2, HALF, *a.shape[1:])


def body(
    tokens, seq_lengths, block_picks, w_query, w_key, w_value, w_gate, w_ckey, w_cvalue, w_out
):
    x = tokens[0]
    kv, tp, dp = lax.axis_index("kv"), lax.axis_index("tp"), lax.axis_index("dp")
    piece = jnp.concatenate(
        [
            w_query[:, :256],
            w_key[:, :64],
            w_value[:, :64],
            w_query[:, 256:],
            w_key[:, 64:],
            w_value[:, 64:],
        ],
        axis=1,
    )
    w_all = gather_weights(piece).reshape(2048, 768)
    out_w = lax.all_gather(w_out, "kv", axis=1, tiled=True)
    out_w = lax.all_gather(out_w, "tp", axis=0, tiled=True)

    gate_all = jax.nn.sigmoid(jnp.dot(x, w_gate, preferred_element_type=jnp.float32))
    gate_all = gate_all.reshape(384, 2, 2, 2, PER)
    gate_own = lax.dynamic_index_in_dim(gate_all, tp, 2, keepdims=False)
    gate_own = gate_own.transpose(2, 1, 3, 0).reshape(2, 8, 2, HALF).transpose(0, 2, 1, 3)
    hi = gate_own.astype(jnp.bfloat16)
    lo = (gate_own - hi.astype(jnp.float32)).astype(jnp.bfloat16)
    gate_rows = jnp.concatenate([hi, lo], axis=2)
    gate_rows = jnp.pad(gate_rows, ((0, 0), (0, 0), (0, 0), (0, 64)))

    qkv = jnp.dot(x, w_all, preferred_element_type=jnp.float32).astype(jnp.bfloat16)
    mains = []
    for gl in range(2):
        one = qkv[:, gl * 384 : (gl + 1) * 384]
        ck = jnp.dot(
            one[:, 256:320].reshape(6, BLK * HEAD), w_ckey, preferred_element_type=jnp.float32
        )
        cv = jnp.dot(
            one[:, 320:384].reshape(6, BLK * HEAD), w_cvalue, preferred_element_type=jnp.float32
        )
        pairs = jnp.concatenate([ck, cv], axis=1).astype(jnp.bfloat16).reshape(2, 3, 128)
        pairs = jnp.pad(pairs, ((0, 0), (0, 13), (0, 0)))
        extra = jnp.concatenate([gate_rows[gl], pairs], axis=2)
        mains.append(jnp.concatenate([by_halves(one), extra], axis=1))
    main = jnp.stack(mains)

    picks = block_picks[0].transpose(1, 0, 2).reshape(2, 2, 3, PICKS)
    ints = jnp.pad(picks, ((0, 0), (0, 0), (0, 5), (0, 112)))
    row = lax.broadcasted_iota(jnp.int32, ints.shape, 2)
    ints = jnp.where(row == 7, seq_lengths[0], ints)

    got, gint = spread(main, ints)
    lens = gint[:, 7, 0]
    ids = jnp.arange(4, dtype=jnp.int32)
    ahead = (lens[None, :] > lens[:, None]) | (
        (lens[None, :] == lens[:, None]) & (ids[None, :] < ids[:, None])
    )
    rank = jnp.sum(ahead.astype(jnp.int32), axis=1)
    order = jnp.sum(jnp.where(rank[None, :] == ids[:, None], ids[None, :], 0), axis=1)
    ranked = jnp.sum(
        jnp.where(rank[None, :] == ids[:, None], lens[None, :], 0), axis=1
    )
    pieces = got[:, :, 256:384]
    src = jnp.stack([lax.dynamic_index_in_dim(pieces, order[r], 0, keepdims=False) for r in range(4)])
    sel = gint[:, :3, :PICKS]
    bias = jnp.repeat((sel >= 0).astype(jnp.float32), BLK, axis=2).reshape(4, 3, 1, PICKS * BLK)
    both_parts = got[:, HALF:ROWS, :HALF].astype(jnp.float32)
    gates = (both_parts[:, :8] + both_parts[:, 8:]).transpose(0, 2, 1)

    def run(spans, number):
        gathered = gather_kv(src, spans, number)
        comp = []
        for rows, g in zip(spans, gathered):
            c = g[:, :, :, HALF : HALF + 3].reshape(2, rows * N, 3, 128)
            c = c.transpose(1, 0, 2, 3).reshape(rows * N * 6, 128)
            at = jnp.arange(rows * N * 6, dtype=jnp.int32)[:, None] // 6
            c = jnp.where(at <= kv, c, jnp.zeros_like(c))
            comp.append(jnp.pad(c, ((0, 384 - rows * N * 6), (0, 0))))
        return attend(spans, order, lens, sel, got, gates, bias, jnp.stack(comp), gathered)

    span = N * 384
    small = (ranked[1] <= 3 * span) & (ranked[2] <= 2 * span)
    att = lax.cond(small, lambda: run((8, 3, 2, 2), 2), lambda: run((8, 8, 8, 8), 3))

    back = lax.all_to_all(att, "dp", split_axis=0, concat_axis=0, tiled=True)
    summed = jnp.zeros((HALF, 2048), jnp.float32)
    for s in range(2):
        cols = jnp.concatenate([back[2 * s], back[2 * s + 1]], axis=1)
        summed = summed + jnp.dot(
            cols, out_w[s * 512 : (s + 1) * 512], preferred_element_type=jnp.float32
        ).astype(jnp.bfloat16).astype(jnp.float32)
    spots = kv * 384 + tp * HALF + jnp.arange(HALF, dtype=jnp.int32)
    alive = spots < seq_lengths[0]
    return jnp.where(alive[:, None], summed, 0.0).astype(jnp.bfloat16)[None]


def solution(mesh):
    return jax.shard_map(
        body,
        mesh=mesh,
        in_specs=(
            P("dp", "kv", None),
            P("dp"),
            P("dp", "kv", "tp", None),
            P("kv", "tp"),
            P("kv", "tp"),
            P("kv", "tp"),
            P(),
            P(),
            P(),
            P("tp", "kv"),
        ),
        out_specs=P("dp", ("kv", "tp"), None),
        check_vma=False,
    )
```

time: 317 us -> 262 us (0.83)
  the two profiles are of different devices: /device:TPU:87 before, /device:TPU:1 now
where the time goes in v1:
time: 262 us; the launch traced here: 261 us
  Pallas kernels  145 us (55%)
  waiting for transfers between devices  47.1 us (18%)
  local copies, waits for them, and re-layouts  25.6 us (10%)
  between operations  23.1 us (9%)
  matrix products  12.3 us (5%)
  other arithmetic  4.38 us (2%)
  starting transfers between devices  3.51 us (1%)
    pallas_call x1, Pallas kernels, gather_kv(): pl.pallas_call(functools.partial(kv_kernel, spans), out_shape=[jax.ShapeD...  55.4 us
    pallas_call x1, Pallas kernels, gather_weights(): pl.pallas_call(weights_kernel, out_shape=jax.ShapeDtypeStruct((N, N, rows...  41.4 us
    all_gather x1, waiting for transfers between devices, body(): out_w = lax.all_gather(w_out, 'kv', axis=1, tiled=True)  38.6 us
    pallas_call x1, Pallas kernels, attend(): pl.pallas_call(functools.partial(attend_kernel, spans), out_shape=jax.Sha...  30.5 us
    pallas_call x1, Pallas kernels, spread(): pl.pallas_call(spread_kernel, out_shape=[jax.ShapeDtypeStruct((4,) + main...  17.9 us
    cond x18, local copies, waits for them, and re-layouts  14.5 us
    all_to_all x1, waiting for transfers between devices, body(): back = lax.all_to_all(att, 'dp', split_axis=0, concat_axis=0, tiled=True)  7.76 us
    dot_general x2, matrix products, body(): jnp.dot(cols, out_w[s * 512:(s + 1) * 512], preferred_element_type=jnp.fl...  5.75 us
  transfers between devices with their start and end apart: 3, of which 2 were waited for; matrix products, arithmetic and copies ran while one was open for 8% of the time, Pallas kernels for 56%

profile of v1, /device:TPU:1, one launch (start us, length us, event | category | flops | bytes accessed | tf_op | source)
XLA Modules:
  0.0 261.4 jit_solution(3612962925255147609)
XLA Ops:
  7.3 0.7 fusion.67
  8.0 0.9 fusion.68
  9.0 41.4 %gather_weights.1 = bf16[8,8,32,768]{3,2,1,0:T(8,128)(2,1)S(1)} custom-call(bf16[32,768]{1,0:T(8,128)(2,1)S(1)} %concatenate.34.src_ref), custom_call_target="tpu_custom_call" | custom-call | tf_op jit(solution)/shard_map/gather_weights/pallas_call | solution.py:286
  50.4 1.8 fusion.25
  55.3 1.3 convolution_convert_fusion.4
  56.6 38.6 %all-gather.3.cloned.1.call-done = bf16[512,2048]{0,1:T(8,128)(2,1)} async-done(((bf16[512,32]{0,1:T(8,128)(2,1)}), bf16[512,2048]{0,1:T(8,128)(2,1)}) %all-gather.3.cloned.1.call-update) | async-done | bytes 2097168 | tf_op jit(solution)/shard_map/all_gather | solution.py:564
  95.2 1.3 convolution_convert_fusion.5
  96.9 1.3 convolution_convert_fusion.3
  98.6 17.9 %spread.1 = (bf16[4,208,384]{2,1,0:T(8,128)(2,1)S(1)}, s32[4,8,128]{2,1,0:T(8,128)S(1)}) custom-call(bf16[2,2,208,384]{3,2,1,0:T(8,128)(2,1)S(1)} %pad_maximum_fusion.2.main_ref, s32[2,2,8,128]{3,2,1,0:T(8,128)S(1)} %pad_select_fusion.ints_ref), custom_call_target="tpu_custom_call" | custom-call | tf_op jit(solution)/shard_map/spread/pallas_call | solution.py:367
  128.0 109.5 %conditional.1 = (bf16[4,192,256]{2,1,0:T(8,128)(2,1)}) conditional(s32[]{:T(128)} %bitcast.37, (s32[]{:T(128)}, bf16[4,208,128]{2,1,0:T(8,128)(2,1)S(1)}, s32[4]{0:T(128)S(1)}, s32[4]{0:T(128)S(1)}, s32[4,3,16]{2,1,0:T(4,128)S(1)}, /*index=5*/bf16[4,208,384]{2,1,0:T(8,128)(2,1)S(1)}, f32[4,192,8]{1,2,0:T(8,128)}, ...), branch_computations={%region_3.4_spmd, %region_4.5_spmd} | conditional | flops 789888 | bytes 140297120 | solution.py:628
  128.0 0.8 copy-done.14
  128.9 55.4 %gather_kv.3 = (bf16[2,8,8,208,128]{4,3,2,1,0:T(8,128)(2,1)S(1)}, bf16[2,3,8,208,128]{4,3,2,1,0:T(8,128)(2,1)S(1)}, bf16[2,2,8,208,128]{4,3,2,1,0:T(8,128)(2,1)S(1)}, bf16[2,2,8,208,128]{4,3,2,1,0:T(8,128)(2,1)S(1)}) custom-call(bf16[4,208,128]{2,1,0:T(8,128)(2,1)S(1)} %get-tuple-element.59.src_ref), custom_call_target="tpu_custom_call" | custom-call | tf_op jit(solution)/shard_map/cond/branch_1_fun/gather_kv/pallas_call | solution.py:419
  184.2 2.8 %copy-done.1 = bf16[2,8,8,208,128]{4,3,2,1,0:T(8,128)(2,1)} copy-done((bf16[2,8,8,208,128]{4,3,2,1,0:T(8,128)(2,1)}, bf16[2,8,8,208,128]{4,3,2,1,0:T(8,128)(2,1)S(1)}, u32[]{:S(2)}) %copy-start.1) | copy-done | bytes 6815768 | tf_op jit(solution)/shard_map/cond
  187.0 1.5 copy-done.8
  188.6 1.2 copy-done.10
  189.8 0.9 slice.91
  191.5 1.0 slice.88
  192.6 0.7 reshape.331
  193.3 1.0 broadcast_select_fusion.4
  194.3 0.9 slice.89
  195.4 1.7 pad_maximum_fusion.1.comp_ref
  197.2 1.7 copy.61.gate_ref
  198.9 2.9 %copy-done.2 = bf16[2,8,8,208,128]{4,3,2,1,0:T(8,128)(2,1)S(1)} copy-done((bf16[2,8,8,208,128]{4,3,2,1,0:T(8,128)(2,1)S(1)}, bf16[2,8,8,208,128]{4,3,2,1,0:T(8,128)(2,1)}, u32[]{:S(2)}) %copy-start.2) | copy-done | bytes 6815768 | tf_op jit(solution)/shard_map/cond
  201.8 1.7 copy-done.9
  203.5 1.5 copy-done.11
  205.0 1.0 copy-done.12
  206.0 1.0 copy-done.13
  207.0 30.5 %attend.3 = bf16[4,192,256]{2,1,0:T(8,128)(2,1)} custom-call(s32[4]{0:T(128)S(1)} %get-tuple-element.52.order_ref, s32[4]{0:T(128)S(1)} %get-tuple-element.53.lens_ref, s32[4,3,16]{2,1,0:T(4,128)S(1)} %get-tuple-element.54.picks_ref, bf16[4,208,384]{2,1,0:T(8,128)(2,1)} %copy-done.14, f32[4,192,8]{2,1,0:T(8,128)S(1)} %copy-done.13, ...), custom_call_target="tpu_custom_call" | custom-call | tf_op jit(solution)/shard_map/cond/branch_1_fun/attend/pallas_call | solution.py:529
  237.5 3.5 %all-to-all-start = ((bf16[4,192,256]{2,1,0:T(8,128)(2,1)}), bf16[4,192,256]{2,1,0:T(8,128)(2,1)S(1)}, u32[]{:S(2)}, u32[]{:S(2)}) async-start(bf16[4,192,256]{2,1,0:T(8,128)(2,1)} %get-tuple-element.156), calls=%async_computation | async-start | bytes 786432 | tf_op jit(solution)/shard_map/all_to_all | solution.py:630
  241.0 7.8 %all-to-all-done = bf16[4,192,256]{2,1,0:T(8,128)(2,1)S(1)} async-done(((bf16[4,192,256]{2,1,0:T(8,128)(2,1)}), bf16[4,192,256]{2,1,0:T(8,128)(2,1)S(1)}, u32[]{:S(2)}, u32[]{:S(2)}) %all-to-all-start) | async-done | bytes 393248 | tf_op jit(solution)/shard_map/all_to_all | solution.py:630
  248.8 2.4 fusion.14
  251.3 3.3 %fusion.15 = bf16[1,192,2048]{2,1,0:T(8,128)(2,1)} fusion(f32[192,2048]{1,0:T(8,128)S(1)} %fusion.14, bf16[1024,2048]{0,1:T(8,128)(2,1)} %all-gather.5.cloned.1.call-done, pred[192]{0:T(512)(128)(4,1)S(1)} %add_compare_fusion, bf16[192,256]{1,0:T(8,128)(2,1)S(1)} %get-tuple-element.133, bf16[192,256]{1,0:T(8,128)(2,1)S(1)} %get-tuple-element.132), kind=kOutput, calls=%fused_computation.54 | convolution fusion | flops 405012480 | bytes 4653248 | tf_op jit(solution)/shard_map/dot_general | solution.py:634
  (83 shorter events, 7.7 us)
Async XLA Ops:
  6.5 43.9 %copy-start = (bf16[1,384,2048]{2,1,0:T(8,128)(2,1)S(1)}, bf16[1,384,2048]{2,1,0:T(8,128)(2,1)}, u32[]{:S(2)}) copy-start(bf16[1,384,2048]{2,1,0:T(8,128)(2,1)} %param.12) | copy-start | bytes 4718596
  6.5 88.7 %all-gather.3.cloned.1.call-start = ((), (), s32[]{:S(2)}) async-start(), calls=%async_computation.1 | async-start | bytes 2129920 | tf_op jit(solution)/shard_map/all_gather | solution.py:564
  7.3 241.6 %all-gather.5.cloned.1.call-start = ((), (), s32[]{:S(2)}) async-start(), calls=%async_computation.2 | async-start | bytes 6291456 | tf_op jit(solution)/shard_map/all_gather | solution.py:565
  50.4 2.4 copy-start.15
  52.8 2.5 copy-start.16
  54.3 42.4 %copy-start.17 = (bf16[4096,64]{0,1:T(8,128)(2,1)S(1)}, bf16[4096,64]{0,1:T(8,128)(2,1)}, u32[]{:S(2)}) copy-start(bf16[4096,64]{0,1:T(8,128)(2,1)} %param.20) | copy-start | bytes 1572868
  128.0 0.8 copy-start.14
  184.2 2.8 %copy-start.1 = (bf16[2,8,8,208,128]{4,3,2,1,0:T(8,128)(2,1)}, bf16[2,8,8,208,128]{4,3,2,1,0:T(8,128)(2,1)S(1)}, u32[]{:S(2)}) copy-start(bf16[2,8,8,208,128]{4,3,2,1,0:T(8,128)(2,1)S(1)} %get-tuple-element.60.refs_0_) | copy-start | bytes 20447236 | tf_op jit(solution)/shard_map/cond
  187.0 1.5 copy-start.8
  188.6 1.2 copy-start.10
  198.9 2.9 %copy-start.2 = (bf16[2,8,8,208,128]{4,3,2,1,0:T(8,128)(2,1)S(1)}, bf16[2,8,8,208,128]{4,3,2,1,0:T(8,128)(2,1)}, u32[]{:S(2)}) copy-start(bf16[2,8,8,208,128]{4,3,2,1,0:T(8,128)(2,1)} %copy-done.1) | copy-start | bytes 20447236 | tf_op jit(solution)/shard_map/cond
  201.8 1.7 copy-start.9
  203.5 1.5 copy-start.11
  205.0 1.0 copy-start.12
  206.0 1.0 copy-start.13
  237.5 11.3 %all-to-all-start = ((bf16[4,192,256]{2,1,0:T(8,128)(2,1)}), bf16[4,192,256]{2,1,0:T(8,128)(2,1)S(1)}, u32[]{:S(2)}, u32[]{:S(2)}) async-start(bf16[4,192,256]{2,1,0:T(8,128)(2,1)} %get-tuple-element.156), calls=%async_computation | async-start | bytes 786432 | tf_op jit(solution)/shard_map/all_to_all | solution.py:630
Sparse Core Ops, SparseCore 0:
  10.4 84.7 all-gather.2
  97.3 24.3 all-gather.4

commit v2 on v1

v2 whole, which is shorter than its diff:
```python
import functools

import jax
import jax.numpy as jnp
from jax import lax
from jax.experimental import pallas as pl
from jax.experimental.pallas import tpu as pltpu
from jax.sharding import PartitionSpec as P

MESH = pl.DeviceIdType.MESH

HEADS = 16
GROUPS = 4
PER = 4
HEAD = 64
BLK = 64
PICKS = 16
N = 8
ROWS = 208
HALF = 192
SPLIT = 112
MASKED = -1e30
VMEM = pltpu.MemorySpace.VMEM
SMEM = pltpu.MemorySpace.SMEM
HBM = pltpu.MemorySpace.HBM


def place():
    kv = lax.axis_index("kv")
    return kv // N, lax.rem(kv, N)


class Copies:
    def __init__(self, send_sems, recv_sems):
        self.send_sems, self.recv_sems, self.used, self.sent = send_sems, recv_sems, 0, []

    def slot(self):
        self.used += 1
        return self.used - 1

    def send(self, i, src, dst, device):
        copy = pltpu.make_async_remote_copy(
            src_ref=src,
            dst_ref=dst,
            send_sem=self.send_sems.at[i],
            recv_sem=self.recv_sems.at[i],
            device_id=device,
            device_id_type=MESH,
        )
        copy.start()

    def arrived(self, i, ref, device):
        pltpu.make_async_remote_copy(
            src_ref=ref,
            dst_ref=ref,
            send_sem=self.send_sems.at[i],
            recv_sem=self.recv_sems.at[i],
            device_id=device,
            device_id_type=MESH,
        ).wait_recv()

    def left(self, i, ref, device):
        pltpu.make_async_remote_copy(
            src_ref=ref,
            dst_ref=ref,
            send_sem=self.send_sems.at[i],
            recv_sem=self.recv_sems.at[i],
            device_id=device,
            device_id_type=MESH,
        ).wait_send()


def when(cond, fn):
    if cond is True:
        fn()
    elif cond is not False:
        pl.when(cond)(fn)


def both(a, b):
    if a is True:
        return b
    if b is True:
        return a
    if a is False or b is False:
        return False
    return jnp.logical_and(a, b)


def wrap(i):
    return lax.rem(i + N, N)


def barrier(kinds):
    sem = pltpu.get_barrier_semaphore()
    for device in kinds:
        pl.semaphore_signal(sem, inc=1, device_id=device, device_id_type=MESH)
    pl.semaphore_wait(sem, len(kinds))


def plane_partners(z, y):
    return [{"kv": z * N + wrap(y + d)} for d in range(1, N)] + [
        {"kv": wrap(z + d) * N + y} for d in range(1, N)
    ]


class Gather:
    def __init__(self, copies, src, view, rows, causal, pair, parts=(True, True), tie=False):
        self.c, self.src, self.view, self.rows, self.causal = copies, src, view, rows, causal
        self.pair, self.parts, self.tie = pair, parts, tie
        self.z, self.y = place()
        self.live = True if rows == N else self.z < rows
        self.waits = []
        self.pair_waits = []
        self.flight = {}
        if not causal:
            self.subs_b = [(0, 4), (4, 4)]
        elif rows == N:
            self.subs_b = [(0, 1), (1, 1), (2, 2), (4, 2), (6, 2)]
        else:
            self.subs_b = [(i, 1) for i in range(rows)]

    def dev(self, z, y):
        return {"kv": z * N + y}

    def transfer(self, cond_send, src, dst, device, cond_recv, got):
        i = self.c.slot()
        when(cond_send, lambda: self.c.send(i, src, dst, device))
        self.waits.append((i, cond_send, src, device))
        return (i, cond_recv, got, device)

    def take(self, t):
        i, cond, ref, device = t
        when(cond, lambda: self.c.arrived(i, ref, device))

    def mirror(self, cond, ref):
        if self.pair is None:
            return
        i = self.c.slot()
        when(cond, lambda: self.c.send(i, ref, ref, self.pair))
        self.pair_waits.append((i, cond, ref))

    def first(self):
        z, y = self.z, self.y
        self.a1, self.b1 = [], []
        for d in range(1, N) if self.parts[0] else ():
            self.a1.append(
                self.transfer(
                    self.live,
                    self.src(0),
                    self.view(z, 1, y, 1, 0),
                    self.dev(z, wrap(y + d)),
                    self.live,
                    self.view(z, 1, wrap(y - d), 1, 0),
                )
            )
        reach = N if not self.causal else self.rows
        for d in range(1, reach) if self.parts[1] else ():
            cs = True if not self.causal else z + d < self.rows
            cr = True if not self.causal else both(self.live, z - d >= 0)
            self.b1.append(
                self.transfer(
                    cs,
                    self.src(1),
                    self.view(z, 1, y, 1, 1),
                    self.dev(wrap(z + d), y),
                    cr,
                    self.view(wrap(z - d), 1, y, 1, 1),
                )
            )

    def ring_y(self, k, z0, nz, part, right, cond):
        z, y = self.z, self.y
        if right:
            o, got, to = wrap(y - (k - 1)), wrap(y - k), wrap(y + 1)
        else:
            o, got, to = lax.rem(y + k - 1, N), lax.rem(y + k, N), wrap(y - 1)
        return self.transfer(
            cond,
            self.view(z0, nz, o, 1, part),
            self.view(z0, nz, o, 1, part),
            self.dev(z, to),
            cond,
            self.view(z0, nz, got, 1, part),
        )

    def hop_a(self, right, sub, k, depth):
        z, y = self.z, self.y
        y0, ny = (sub * 4, 4)
        if right:
            o, got, to = wrap(z - (k - 1)), wrap(z - k), wrap(z + 1)
            cs = both(z - (k - 1) >= 0, z + 1 < self.rows) if self.causal else True
            cr = both(self.live, z - k >= 0) if self.causal else True
        else:
            o, got, to = wrap(z + k - 1), lax.rem(z + k, N), wrap(z - 1)
            cs = o < depth if self.causal else True
            cr = got < depth if self.causal else True
        return self.transfer(
            cs,
            self.view(o, 1, y0, ny, 0),
            self.view(o, 1, y0, ny, 0),
            self.dev(to, y),
            cr,
            self.view(got, 1, y0, ny, 0),
        )

    def hop_b(self, right, sub, k):
        z0, nz = self.subs_b[sub]
        cond = self.live
        if self.causal and z0 > 0:
            cond = both(cond, self.z >= z0)
        return self.ring_y(k, z0, nz, 1, right, cond)

    def depth_a(self, right, sub):
        if self.rows < N:
            return self.rows - 1 if right else 0
        return 4 if right == (sub == 0) else 3

    def depth_b(self, right, sub):
        return 4 if right == ((sub % 2 == 0) != self.tie) else 3

    def hop(self, k):
        steps = []
        order = [("a", 0), ("b", 0), ("b", 1), ("a", 1)] + [("b", i) for i in range(2, 5)]
        begun = set()
        for ring, s in order:
            if s >= (2 if ring == "a" else len(self.subs_b)) or not self.parts[ring == "b"]:
                continue
            if k == 1 and ring not in begun:
                begun.add(ring)
                steps.append(lambda ring=ring: self.begin(ring))
            for r in (True, False):
                steps.append(lambda ring=ring, s=s, r=r: self.lane(ring, s, r, k))
        return steps

    def begin(self, ring):
        for t in self.a1 if ring == "a" else self.b1:
            self.take(t)

    def lane(self, ring, s, r, k):
        depth = self.depth_a(r, s) if ring == "a" else self.depth_b(r, s)
        got = None
        if 1 < k <= depth + 1:
            got = self.flight[ring, r, s]
            self.take(got)
        if k <= depth:
            self.flight[ring, r, s] = (
                self.hop_a(r, s, k, depth) if ring == "a" else self.hop_b(r, s, k)
            )
        if got is not None:
            self.mirror(got[1], got[2])
        if k == 1 and r:
            if ring == "a":
                self.mirror(self.live, self.view(self.z, 1, s * 4, 4, 0))
            else:
                z0, nz = self.subs_b[s]
                cond = both(self.live, self.z >= z0) if z0 else self.live
                self.mirror(cond, self.view(z0, nz, self.y, 1, 1))

    def last(self):
        for i, cond, ref in self.pair_waits:
            when(cond, lambda: self.c.arrived(i, ref, self.pair))
            when(cond, lambda: self.c.left(i, ref, self.pair))
        for i, cond, ref, device in self.waits:
            when(cond, lambda: self.c.left(i, ref, device))


def weights_kernel(*refs):
    srcs, outs, (send_sems, recv_sems) = refs[:2], refs[2:4], refs[4:]
    z, y = place()
    for src_ref, out_ref in zip(srcs, outs):
        out_ref[z, y] = src_ref[...]
    barrier(plane_partners(z, y))
    c = Copies(send_sems, recv_sems)
    jobs = []
    for src_ref, out_ref in zip(srcs, outs):
        half = src_ref.shape[0] // 2

        def src(part, src_ref=src_ref, half=half):
            return src_ref.at[pl.ds(part * half, half)]

        def view(z0, nz, y0, ny, part, out_ref=out_ref, half=half):
            zi = z0 if nz == 1 else pl.ds(z0, nz)
            yi = y0 if ny == 1 else pl.ds(y0, ny)
            return out_ref.at[zi, yi, pl.ds(part * half, half)]

        jobs.append(Gather(c, src, view, N, False, None))
    for g in jobs:
        g.first()
    for k in range(1, 6):
        for g in jobs:
            for step in g.hop(k):
                step()
    for g in jobs:
        g.last()


def gather_weights(*pieces):
    vm = pl.BlockSpec(memory_space=VMEM)
    return pl.pallas_call(
        weights_kernel,
        out_shape=[jax.ShapeDtypeStruct((N, N) + p.shape, p.dtype) for p in pieces],
        in_specs=[vm, vm],
        out_specs=[vm, vm],
        scratch_shapes=[pltpu.SemaphoreType.DMA((96,)), pltpu.SemaphoreType.DMA((96,))],
        compiler_params=pltpu.CompilerParams(
            collective_id=0, has_side_effects=True, vmem_limit_bytes=24 << 20
        ),
        name="gather_weights",
    )(*pieces)


def spread_partners(dp, tp):
    return [
        {"dp": lax.rem(dp + e // 2, 4), "tp": lax.rem(tp + e % 2, 2)} for e in range(1, 8)
    ]


def spread_kernel(main_ref, ints_ref, got_ref, gint_ref, send_sems, recv_sems):
    dp, tp = lax.axis_index("dp"), lax.axis_index("tp")
    barrier(spread_partners(dp, tp))
    pairs = ((main_ref, got_ref), (ints_ref, gint_ref))

    def copy(gl, h, k):
        s, d = pairs[k]
        return pltpu.make_async_remote_copy(
            src_ref=s.at[gl, h],
            dst_ref=d.at[dp],
            send_sem=send_sems.at[(gl * 2 + h) * 2 + k],
            recv_sem=recv_sems.at[dp, k],
            device_id={"dp": 2 * tp + gl, "tp": jnp.int32(h)},
            device_id_type=MESH,
        )

    def is_own(gl, h):
        return jnp.logical_and(2 * tp + gl == dp, tp == h)

    for gl in range(2):
        for h in range(2):

            def go(gl=gl, h=h):
                for k in range(2):
                    copy(gl, h, k).start()

            def keep(gl=gl, h=h):
                got_ref[dp] = main_ref[gl, h]
                gint_ref[dp] = ints_ref[gl, h]

            pl.when(jnp.logical_not(is_own(gl, h)))(go)
            pl.when(is_own(gl, h))(keep)
    for q in range(4):

        def take(q=q):
            for k, d in enumerate((got_ref, gint_ref)):
                pltpu.make_async_remote_copy(
                    src_ref=d.at[q],
                    dst_ref=d.at[q],
                    send_sem=send_sems.at[k],
                    recv_sem=recv_sems.at[q, k],
                    device_id={"dp": jnp.int32(q), "tp": tp},
                    device_id_type=MESH,
                ).wait_recv()

        pl.when(jnp.logical_not(jnp.logical_and(q == dp, dp // 2 == tp)))(take)
    for gl in range(2):
        for h in range(2):

            def done(gl=gl, h=h):
                for k in range(2):
                    copy(gl, h, k).wait_send()

            pl.when(jnp.logical_not(is_own(gl, h)))(done)


def spread(main, ints):
    return pl.pallas_call(
        spread_kernel,
        out_shape=[
            jax.ShapeDtypeStruct((4,) + main.shape[2:], main.dtype),
            jax.ShapeDtypeStruct((4,) + ints.shape[2:], ints.dtype),
        ],
        in_specs=[pl.BlockSpec(memory_space=VMEM)] * 2,
        out_specs=[pl.BlockSpec(memory_space=VMEM)] * 2,
        scratch_shapes=[pltpu.SemaphoreType.DMA((8,)), pltpu.SemaphoreType.DMA((4, 2))],
        compiler_params=pltpu.CompilerParams(
            collective_id=1, has_side_effects=True, vmem_limit_bytes=16 << 20
        ),
        name="spread",
    )(main, ints)


def bases(spans):
    return [sum(spans[:r]) for r in range(4)]


def kv_kernel(spans, order_ref, got_ref, w_ref, out_ref, wo_ref, own, send_sems, recv_sems):
    z, y = place()
    tp, dp = lax.axis_index("tp"), lax.axis_index("dp")
    pair = {"tp": 1 - tp}
    base = bases(spans)
    for r, rows in enumerate(spans):

        def fill(r=r):
            piece = got_ref[order_ref[r], :, pl.ds(PER * HEAD, 2 * HEAD)]
            own[r] = piece
            out_ref[tp, base[r] + z, y] = piece

        when(True if rows == N else z < rows, fill)
    left, right = lax.rem(dp + 3, 4), lax.rem(dp + 1, 4)
    barrier(plane_partners(z, y) + [pair, {"dp": left}, {"dp": right}])
    c = Copies(send_sems, recv_sems)
    mine = w_ref
    xs = []
    for to in (right, left):
        i = c.slot()
        c.send(i, mine, wo_ref.at[tp, dp], {"dp": to})
        xs.append((i, mine, {"dp": to}))
    i_own = c.slot()
    c.send(i_own, mine, wo_ref.at[tp, dp], pair)
    local = pltpu.make_async_copy(mine, wo_ref.at[tp, dp], send_sems.at[c.slot()])
    local.start()

    jobs = []
    for r, rows in enumerate(spans):

        split = SPLIT if r == 0 else 0

        def part_rows(part, split=split):
            return pl.ds(0, split) if part == 0 else pl.ds(split, ROWS - split)

        def src(part, r=r, part_rows=part_rows):
            return own.at[r, part_rows(part)]

        def view(z0, nz, y0, ny, part, r=r, part_rows=part_rows):
            zi = base[r] + z0 if nz == 1 else pl.ds(base[r] + z0, nz)
            yi = y0 if ny == 1 else pl.ds(y0, ny)
            return out_ref.at[tp, zi, yi, part_rows(part)]

        jobs.append(Gather(c, src, view, rows, True, pair, (r == 0, True), r % 2 == 1))
    for g in jobs:
        g.first()
    mirrors = []
    seconds = []
    for k in range(1, 6):
        for g in jobs:
            for step in g.hop(k):
                step()
        if k == 3:
            for n, (frm, to, half) in enumerate(((left, right, 0), (right, left, 1))):
                i = xs[n][0]
                ref = wo_ref.at[tp, frm]
                c.arrived(i, ref, {"dp": to})
                part = wo_ref.at[tp, frm, pl.ds(half * 4, 4)]
                i2 = c.slot()
                c.send(i2, part, part, {"dp": to})
                seconds.append((i2, part, {"dp": to}, half))
                i3 = c.slot()
                c.send(i3, ref, ref, pair)
                mirrors.append((i3, ref))
    far = lax.rem(dp + 2, 4)
    for i2, part, to, half in seconds:
        ref = wo_ref.at[tp, far, pl.ds(half * 4, 4)]
        c.arrived(i2, ref, to)
        i3 = c.slot()
        c.send(i3, ref, ref, pair)
        mirrors.append((i3, ref))
    assert c.used <= send_sems.shape[0], c.used
    for g in jobs:
        g.last()
    c.arrived(i_own, wo_ref.at[tp, dp], pair)
    c.left(i_own, mine, pair)
    for i, ref in mirrors:
        c.arrived(i, ref, pair)
        c.left(i, ref, pair)
    for i, ref, to in xs:
        c.left(i, ref, to)
    for i2, part, to, half in seconds:
        c.left(i2, part, to)
    local.wait()


def gather_kv(order, got, w_part, spans, number, limit):
    vm = pl.BlockSpec(memory_space=VMEM)
    return pl.pallas_call(
        functools.partial(kv_kernel, spans),
        out_shape=[
            jax.ShapeDtypeStruct((2, sum(spans), N, ROWS, 2 * HEAD), got.dtype),
            jax.ShapeDtypeStruct((2, 4, N, N, 32, 128), got.dtype),
        ],
        in_specs=[pl.BlockSpec(memory_space=SMEM), vm, pl.BlockSpec(memory_space=HBM)],
        out_specs=[vm, vm],
        scratch_shapes=[
            pltpu.VMEM((4, ROWS, 2 * HEAD), jnp.bfloat16),
            pltpu.SemaphoreType.DMA((limit,)),
            pltpu.SemaphoreType.DMA((limit,)),
        ],
        compiler_params=pltpu.CompilerParams(
            collective_id=number,
            has_side_effects=True,
            vmem_limit_bytes=(24 if sum(spans) < 20 else 56) << 20,
        ),
        name="gather_kv",
    )(order, got, w_part)


def attend_kernel(spans, order_ref, ints_ref, main_ref, kv_ref, block_ref, out_ref, buf, comp, gates):
    kv, tp = lax.axis_index("kv"), lax.axis_index("tp")
    start = kv * (2 * HALF) + tp * HALF
    base = bases(spans)
    lane = lax.broadcasted_iota(jnp.int32, (BLK, 128), 1)
    row_in = lax.rem(lax.broadcasted_iota(jnp.int32, (PER * BLK, 1), 0), BLK)
    comp[...] = jnp.zeros_like(comp)
    to_row = lax.broadcasted_iota(jnp.int32, (48, 256), 0)
    from_row = lax.broadcasted_iota(jnp.int32, (48, 256), 1)
    piece = (to_row * 21846) >> 16
    pick_rows = jnp.where(from_row == piece * 16 + (to_row - piece * 3), 1.0, 0.0).astype(jnp.bfloat16)
    turn = jnp.where(
        lax.rem(lax.broadcasted_iota(jnp.int32, (16, 128), 0), 8)
        == lax.broadcasted_iota(jnp.int32, (16, 128), 1),
        1.0,
        0.0,
    ).astype(jnp.bfloat16)
    block_ends = block_ref[...] * BLK + (BLK - 1)

    def step(n, carry):
        r = (n * 21846) >> 16
        j = n - r * 3
        seq = order_ref[r]
        rows = pl.ds(pl.multiple_of(j * BLK, BLK), BLK)
        live = start < ints_ref[seq, 7, 0]
        first = jnp.int32(base[0])
        for q in range(1, 4):
            first = jnp.where(r == q, base[q], first)

        @pl.when(jnp.logical_and(live, j == 0))
        def _():
            def pack(z, carry):
                tile = kv_ref[:, first + z, :, pl.ds(HALF, 16), :].reshape(256, 128)
                got = jnp.dot(pick_rows, tile, preferred_element_type=jnp.float32)
                comp[pl.ds(pl.multiple_of(z * 48, 16), 48), :] = got.astype(jnp.bfloat16)
                return carry

            lax.fori_loop(0, kv // N + 1, pack, 0)
            gates[...] = lax.dot_general(
                main_ref[seq, pl.ds(HALF, 16), pl.ds(0, HALF + 64)],
                turn,
                (((0,), (0,)), ((), ())),
                preferred_element_type=jnp.float32,
            )

        @pl.when(jnp.logical_not(live))
        def _():
            out_ref[seq, rows] = jnp.zeros((BLK, PER * HEAD), jnp.bfloat16)

        @pl.when(live)
        def _():
            def fetch(p, count):
                b = ints_ref[seq, j, p]

                @pl.when(b >= 0)
                def _():
                    span = (b * 10923) >> 16
                    at = b - span * 6
                    t = jnp.where(at >= 3, 1, 0)
                    row = (at - t * 3) * BLK
                    buf[pl.ds(pl.multiple_of(count * BLK, BLK), BLK), :] = kv_ref[
                        t,
                        first + (span >> 3),
                        span & 7,
                        pl.ds(pl.multiple_of(row, BLK), BLK),
                        :,
                    ]

                return count + jnp.where(b >= 0, 1, 0)

            count = lax.fori_loop(0, PICKS, fetch, jnp.int32(0), unroll=True)
            parts = []
            for h in range(PER):
                two = main_ref[seq, rows, pl.ds((h // 2) * 128, 128)].astype(jnp.float32) * 0.125
                if h % 2:
                    two = pltpu.roll(two, 64, 1)
                parts.append(jnp.where(lane < HEAD, two, 0.0).astype(jnp.bfloat16))
            q = jnp.concatenate(parts, axis=0)

            def score(keys):
                return lax.dot_general(
                    q, keys, (((1,), (1,)), ((), ())), preferred_element_type=jnp.float32
                )

            spot = start + j * BLK + row_in
            keys = comp[...]
            seen = block_ends <= spot
            cs = jnp.where(seen, score(keys), MASKED)
            ctop = jnp.max(cs, axis=-1, keepdims=True)
            cw = jnp.exp(cs - ctop)
            cn = jnp.maximum(jnp.sum(cw, axis=-1, keepdims=True), 1.0)
            cp = (cw * jnp.where(spot >= BLK - 1, 1.0 / cn, 0.0)).astype(jnp.bfloat16)
            co = jnp.dot(cp, keys, preferred_element_type=jnp.float32)

            own = main_ref[seq, rows, pl.ds(PER * HEAD, 128)]
            ks = lax.broadcasted_iota(jnp.int32, (1, BLK), 1)

            def finish(so):
                mixed = []
                g = gates[pl.ds(pl.multiple_of(j * BLK, BLK), BLK), :]
                for h in range(PER):
                    at = slice(h * BLK, (h + 1) * BLK)
                    mixed.append(g[:, h : h + 1] * co[at] + g[:, 4 + h : 5 + h] * so[at])
                for h in range(2):
                    pair = jnp.where(
                        lane < HEAD, pltpu.roll(mixed[2 * h], 64, 1), mixed[2 * h + 1]
                    )
                    out_ref[seq, rows, pl.ds(h * 128, 128)] = pair.astype(jnp.bfloat16)

            def own_scores():
                return jnp.where(ks <= row_in, score(own), MASKED)

            @pl.when(count == 0)
            def _():
                os = own_scores()
                ow = jnp.exp(os - jnp.max(os, axis=-1, keepdims=True))
                inv = 1.0 / jnp.sum(ow, axis=-1, keepdims=True)
                finish(jnp.dot((ow * inv).astype(jnp.bfloat16), own, preferred_element_type=jnp.float32))

            @pl.when(count > 0)
            def _():
                os = own_scores()
                far = buf[...]
                spots = lax.broadcasted_iota(jnp.int32, (1, PICKS * BLK), 1)
                fs = jnp.where(spots < count * BLK, score(far), MASKED)
                top = jnp.maximum(
                    jnp.max(os, axis=-1, keepdims=True), jnp.max(fs, axis=-1, keepdims=True)
                )
                ow, fw = jnp.exp(os - top), jnp.exp(fs - top)
                inv = 1.0 / (
                    jnp.sum(ow, axis=-1, keepdims=True) + jnp.sum(fw, axis=-1, keepdims=True)
                )
                so = jnp.dot(
                    (ow * inv).astype(jnp.bfloat16), own, preferred_element_type=jnp.float32
                ) + jnp.dot((fw * inv).astype(jnp.bfloat16), far, preferred_element_type=jnp.float32)
                finish(so)

        return carry

    buf[...] = jnp.zeros_like(buf)
    lax.fori_loop(0, 12, step, 0)


def attend(spans, order, gint, got, gathered):
    vm = pl.BlockSpec(memory_space=VMEM)
    sm = pl.BlockSpec(memory_space=SMEM)
    c = jnp.arange(384, dtype=jnp.int32)
    z, t, y, j = c // 48, c % 48 // 24, c % 24 // 3, c % 3
    blocks = ((z * N + y) * 6 + t * 3 + j)[None]
    return pl.pallas_call(
        functools.partial(attend_kernel, spans),
        out_shape=jax.ShapeDtypeStruct((4, HALF, PER * HEAD), jnp.bfloat16),
        in_specs=[sm, sm, vm, vm, vm],
        out_specs=vm,
        scratch_shapes=[
            pltpu.VMEM((PICKS * BLK, 2 * HEAD), jnp.bfloat16),
            pltpu.VMEM((384, 2 * HEAD), jnp.bfloat16),
            pltpu.VMEM((HALF + 64, 128), jnp.float32),
        ],
        compiler_params=pltpu.CompilerParams(vmem_limit_bytes=(24 if sum(spans) < 20 else 48) << 20),
        name="attend",
    )(order, gint, got, gathered, blocks)


def finish_kernel(len_ref, att_ref, wo_ref, out_ref, back, send_sems, recv_sems):
    dp, kv, tp = lax.axis_index("dp"), lax.axis_index("kv"), lax.axis_index("tp")
    barrier([{"dp": lax.rem(dp + d, 4)} for d in range(1, 4)])

    def copy(d):
        to = lax.rem(dp + d, 4)
        return pltpu.make_async_remote_copy(
            src_ref=att_ref.at[to],
            dst_ref=back.at[dp],
            send_sem=send_sems.at[d],
            recv_sem=recv_sems.at[d],
            device_id={"dp": to},
            device_id_type=MESH,
        )

    for d in (2, 1, 3):
        copy(d).start()
    back[dp] = att_ref[dp]
    for d in (1, 3, 2):
        frm = lax.rem(dp + 4 - d, 4)
        pltpu.make_async_remote_copy(
            src_ref=back.at[frm],
            dst_ref=back.at[frm],
            send_sem=send_sems.at[d],
            recv_sem=recv_sems.at[d],
            device_id={"dp": frm},
            device_id_type=MESH,
        ).wait_recv()
    spot = kv * (2 * HALF) + tp * HALF + lax.broadcasted_iota(jnp.int32, (HALF, 1), 0)
    alive = spot < len_ref[0]
    cols = [jnp.concatenate([back[2 * t], back[2 * t + 1]], axis=1) for t in range(2)]

    def tile(z, carry):
        total = jnp.zeros((HALF, 256), jnp.float32)
        for t in range(2):
            w = jnp.concatenate([wo_ref[t, q, z].reshape(256, 128) for q in range(4)], axis=1)
            part = lax.dot_general(
                cols[t], w, (((1,), (1,)), ((), ())), preferred_element_type=jnp.float32
            )
            total = total + part.astype(jnp.bfloat16).astype(jnp.float32)
        out_ref[:, pl.ds(pl.multiple_of(z * 256, 256), 256)] = jnp.where(alive, total, 0.0).astype(
            jnp.bfloat16
        )
        return carry

    lax.fori_loop(0, N, tile, 0)
    for d in (1, 2, 3):
        copy(d).wait_send()


def finish(length, att, wo, number):
    vm = pl.BlockSpec(memory_space=VMEM)
    return pl.pallas_call(
        finish_kernel,
        out_shape=jax.ShapeDtypeStruct((HALF, 2048), jnp.bfloat16),
        in_specs=[pl.BlockSpec(memory_space=SMEM), vm, vm],
        out_specs=vm,
        scratch_shapes=[
            pltpu.VMEM((4, HALF, PER * HEAD), jnp.bfloat16),
            pltpu.SemaphoreType.DMA((4,)),
            pltpu.SemaphoreType.DMA((4,)),
        ],
        compiler_params=pltpu.CompilerParams(
            collective_id=number, has_side_effects=True, vmem_limit_bytes=24 << 20
        ),
        name="finish",
    )(length, att, wo)


def by_halves(a):
    return a.reshape(2, HALF, *a.shape[1:])


def body(
    tokens, seq_lengths, block_picks, w_query, w_key, w_value, w_gate, w_ckey, w_cvalue, w_out
):
    x = tokens[0]
    kv, tp, dp = lax.axis_index("kv"), lax.axis_index("tp"), lax.axis_index("dp")
    out_part = lax.dynamic_slice_in_dim(w_out.T, dp * 128, 128, axis=1)
    piece = jnp.concatenate(
        [
            w_query[:, :256],
            w_key[:, :64],
            w_value[:, :64],
            w_query[:, 256:],
            w_key[:, 64:],
            w_value[:, 64:],
        ],
        axis=1,
    )
    w_all, w_part = gather_weights(piece, out_part)

    gate_all = jax.nn.sigmoid(jnp.dot(x, w_gate, preferred_element_type=jnp.float32))
    gate_all = gate_all.reshape(384, 2, 2, 2, PER)
    gate_own = lax.dynamic_index_in_dim(gate_all, tp, 2, keepdims=False)
    gate_own = gate_own.transpose(2, 1, 3, 0).reshape(2, 8, 2, HALF).transpose(0, 2, 1, 3)
    hi = gate_own.astype(jnp.bfloat16)
    lo = (gate_own - hi.astype(jnp.float32)).astype(jnp.bfloat16)
    gate_rows = jnp.concatenate([hi, lo], axis=2)
    gate_rows = jnp.pad(gate_rows, ((0, 0), (0, 0), (0, 0), (0, 64)))

    qkv = jnp.dot(x, w_all.reshape(2048, 768), preferred_element_type=jnp.float32).astype(jnp.bfloat16)
    mains = []
    for gl in range(2):
        one = qkv[:, gl * 384 : (gl + 1) * 384]
        ck = jnp.dot(
            one[:, 256:320].reshape(6, BLK * HEAD), w_ckey, preferred_element_type=jnp.float32
        )
        cv = jnp.dot(
            one[:, 320:384].reshape(6, BLK * HEAD), w_cvalue, preferred_element_type=jnp.float32
        )
        pairs = jnp.concatenate([ck, cv], axis=1).astype(jnp.bfloat16).reshape(2, 3, 128)
        pairs = jnp.pad(pairs, ((0, 0), (0, 13), (0, 0)))
        extra = jnp.concatenate([gate_rows[gl], pairs], axis=2)
        mains.append(jnp.concatenate([by_halves(one), extra], axis=1))
    main = jnp.stack(mains)

    picks = block_picks[0].transpose(1, 0, 2).reshape(2, 2, 3, PICKS)
    ints = jnp.pad(picks, ((0, 0), (0, 0), (0, 5), (0, 112)))
    row = lax.broadcasted_iota(jnp.int32, ints.shape, 2)
    ints = jnp.where(row == 7, seq_lengths[0], ints)

    got, gint = spread(main, ints)
    lens = gint[:, 7, 0]
    ids = jnp.arange(4, dtype=jnp.int32)
    ahead = (lens[None, :] > lens[:, None]) | (
        (lens[None, :] == lens[:, None]) & (ids[None, :] < ids[:, None])
    )
    rank = jnp.sum(ahead.astype(jnp.int32), axis=1)
    order = jnp.sum(jnp.where(rank[None, :] == ids[:, None], ids[None, :], 0), axis=1)
    ranked = jnp.sum(
        jnp.where(rank[None, :] == ids[:, None], lens[None, :], 0), axis=1
    )

    def run(spans, number, limit):
        gathered, wo = gather_kv(order, got, w_part, spans, number, limit)
        att = attend(spans, order, gint, got, gathered)
        return finish(seq_lengths, att, wo, number + 1)

    span = N * 384
    small = (ranked[1] <= 3 * span) & (ranked[2] <= 2 * span) & (ranked[3] <= span)
    out = lax.cond(
        small, lambda: run((8, 3, 2, 1), 2, 448), lambda: run((8, 8, 8, 8), 4, 600)
    )
    return out[None]


def solution(mesh):
    return jax.shard_map(
        body,
        mesh=mesh,
        in_specs=(
            P("dp", "kv", None),
            P("dp"),
            P("dp", "kv", "tp", None),
            P("kv", "tp"),
            P("kv", "tp"),
            P("kv", "tp"),
            P(),
            P(),
            P(),
            P("tp", "kv"),
        ),
        out_specs=P("dp", ("kv", "tp"), None),
        check_vma=False,
    )
```

time: 262 us -> 150 us (0.57)
  waiting for transfers between devices: 47.1 us -> 0 us
  between operations: 23.1 us -> 2.86 us
  local copies, waits for them, and re-layouts: 25.6 us -> 7.07 us
  Pallas kernels: 145 us -> 130 us
  matrix products: 12.3 us -> 8.52 us
  starting transfers between devices: 3.51 us -> 0 us
  other arithmetic: 4.38 us -> 0.88 us
    all_gather x2 -> x0, waiting for transfers between devices: 38.6 us -> none  [the longest x1 38.6 us: body(): out_w = lax.all_gather(w_out, 'kv', axis=1, tiled=True)]
    cond x18 -> x0, local copies, waits for them, and re-layouts: 14.5 us -> none
    pallas_call x1, Pallas kernels: 55.4 us -> 41.7 us  [gather_kv(): pl.pallas_call(functools.partial(kv_kernel, spans), out_shape=[jax.ShapeD...]
    pallas_call x1, Pallas kernels: 30.5 us -> 17.7 us  [attend(): pl.pallas_call(functools.partial(attend_kernel, spans), out_shape=jax.Sha...]
    pallas_call x1 -> x2, Pallas kernels: 41.4 us -> 53.9 us  [the longest x1 41.6 us: gather_weights(): pl.pallas_call(weights_kernel, out_shape=[jax.ShapeDtypeStruct((N, N) + p...]
    all_to_all x1 -> x0, waiting for transfers between devices: 7.76 us -> none  [body(): back = lax.all_to_all(att, 'dp', split_axis=0, concat_axis=0, tiled=True)]
    dot_general x3 -> x1, matrix products: 7.58 us -> 1.83 us  [body(): jnp.dot(x, w_all.reshape(2048, 768), preferred_element_type=jnp.float32)]
    all_to_all x1 -> x0, starting transfers between devices: 3.47 us -> none  [body(): back = lax.all_to_all(att, 'dp', split_axis=0, concat_axis=0, tiled=True)]
  transfers between devices with their start and end apart: 3 -> 0, of which waited for: 2 -> 0; matrix products, arithmetic and copies ran while one was open for 8% -> 0% of each run, Pallas kernels for 56% -> 0%
where the time goes in v2:
time: 150 us; the launch traced here: 149 us
  Pallas kernels  130 us (87%)
  matrix products  8.52 us (6%)
  local copies, waits for them, and re-layouts  7.07 us (5%)
  between operations  2.86 us (2%)
    pallas_call x1, Pallas kernels, gather_kv(): pl.pallas_call(functools.partial(kv_kernel, spans), out_shape=[jax.ShapeD...  41.7 us
    pallas_call x1, Pallas kernels, gather_weights(): pl.pallas_call(weights_kernel, out_shape=[jax.ShapeDtypeStruct((N, N) + p...  41.6 us
    pallas_call x1, Pallas kernels, attend(): pl.pallas_call(functools.partial(attend_kernel, spans), out_shape=jax.Sha...  17.7 us
    pallas_call x1, Pallas kernels, spread(): pl.pallas_call(spread_kernel, out_shape=[jax.ShapeDtypeStruct((4,) + main...  16.5 us
    pallas_call x1, Pallas kernels, finish(): pl.pallas_call(finish_kernel, out_shape=jax.ShapeDtypeStruct((HALF, 2048)...  12.3 us

profile of v2, /device:TPU:1, one launch (start us, length us, event | category | flops | bytes accessed | tf_op | source)
XLA Modules:
  0.0 149.4 jit_solution(3637434600678769993)
XLA Ops:
  0.8 0.6 lt.58
  1.4 0.7 dynamic-slice_bitcast_fusion.refs_1_
  2.1 0.7 copy.24
  2.8 0.9 fusion.51
  3.7 0.7 fusion.50
  4.5 1.5 fusion.29
  6.2 41.6 %gather_weights.1 = (bf16[8,8,32,768]{3,2,1,0:T(8,128)(2,1)S(1)}, bf16[8,8,32,128]{3,2,1,0:T(8,128)(2,1)S(1)}) custom-call(bf16[32,768]{1,0:T(8,128)(2,1)S(1)} %concatenate.28.refs_0_, bf16[32,128]{1,0:T(8,128)(2,1)S(1)} %dynamic-slice_bitcast_fusion.refs_1_), custom_call_target="tpu_custom_call" | custom-call | tf_op jit(solution)/shard_map/gather_weights/pallas_call | solution.py:300
  47.9 1.8 %fusion.17 = bf16[384,768]{0,1:T(8,128)(2,1)S(1)} fusion(bf16[2048,768]{1,0:T(8,128)(2,1)S(1)} %bitcast.72, bf16[1,384,2048]{2,1,0:T(8,128)(2,1)S(1)} %copy-done), kind=kOutput, calls=%fused_computation.39 | convolution fusion | flops 1208254464 | bytes 5308416 | tf_op jit(solution)/shard_map/dot_general | solution.py:771
  49.8 0.2 copy.16
  50.0 0.1 copy.19
  50.2 0.1 dot_general.28
  50.3 1.3 convolution_convert_fusion.3
  51.6 0.1 copy.23
  51.7 0.1 dot_general.34
  51.9 1.3 convolution_convert_fusion
  53.2 0.1 copy.22
  53.3 0.1 dot_general.32
  53.5 1.3 convolution_convert_fusion.1
  54.9 0.1 copy.20
  55.0 0.1 dot_general.30
  55.1 1.3 convolution_convert_fusion.2
  56.6 0.2 copy.21
  56.9 16.5 %spread.1 = (bf16[4,208,384]{2,1,0:T(8,128)(2,1)S(1)}, s32[4,8,128]{2,1,0:T(8,128)S(1)}) custom-call(bf16[2,2,208,384]{3,2,1,0:T(8,128)(2,1)S(1)} %pad_maximum_fusion.main_ref, s32[2,2,8,128]{3,2,1,0:T(8,128)S(1)} %pad_select_fusion.ints_ref), custom_call_target="tpu_custom_call" | custom-call | tf_op jit(solution)/shard_map/spread/pallas_call | solution.py:376
  73.5 0.2 slice_reduce_fusion
  73.6 0.2 convert_reduce_fusion
  73.8 0.1 select_reduce_fusion.2
  73.9 0.7 fusion.53
  76.5 72.1 %conditional.1 = (bf16[1,192,2048]{2,1,0:T(8,128)(2,1)S(1)}) conditional(s32[]{:T(128)} %bitcast.21, (pred[4,4]{1,0:T(4,128)(4,1)S(1)}, s32[4,4]{1,0:T(4,128)S(1)}, bf16[4,208,384]{2,1,0:T(8,128)(2,1)S(1)}, bf16[8,8,32,128]{3,2,1,0:T(8,128)(2,1)S(1)}, s32[4,8,128]{2,1,0:T(8,128)S(1)}, /*index=5*/s32[1]{0:T(128)}) %tuple.30, ...), branch_computations={%region_2.4_spmd, %region_4.6_spmd} | conditional | flops 17692 | bytes 16778976 | solution.py:811
  76.8 41.7 %gather_kv.3 = (bf16[2,14,8,208,128]{4,3,2,1,0:T(8,128)(2,1)S(1)}, bf16[2,4,8,8,32,128]{5,4,3,2,1,0:T(8,128)(2,1)S(1)}) custom-call(s32[4]{0:T(128)S(1)} %select_reduce_fusion.1.order_ref, bf16[4,208,384]{2,1,0:T(8,128)(2,1)S(1)} %get-tuple-element.55.got_ref.main_ref, bf16[8,8,32,128]{3,2,1,0:T(8,128)(2,1)S(1)} %get-tuple-element.56.w_ref), custom_call_target="tpu_custom_call" | custom-call | tf_op jit(solution)/shard_map/cond/branch_1_fun/gather_kv/pallas_call | solution.py:484
  118.5 17.7 %attend.3.att_ref = bf16[4,192,256]{2,1,0:T(8,128)(2,1)S(1)} custom-call(s32[4]{0:T(128)S(1)} %select_reduce_fusion.1.order_ref, s32[4,8,128]{2,1,0:T(8,128)S(1)} %get-tuple-element.54.ints_ref, bf16[4,208,384]{2,1,0:T(8,128)(2,1)S(1)} %get-tuple-element.55.got_ref.main_ref, bf16[2,14,8,208,128]{4,3,2,1,0:T(8,128)(2,1)S(1)} %get-tuple-element.57.kv_ref, ...), custom_call_target="tpu_custom_call" | custom-call | tf_op jit(solution)/shard_map/cond/branch_1_fun/attend/pallas_call | solution.py:655
  136.2 12.3 %finish.3 = bf16[192,2048]{1,0:T(8,128)(2,1)S(1)} custom-call(s32[1]{0:T(128)} %get-tuple-element.51.len_ref, bf16[4,192,256]{2,1,0:T(8,128)(2,1)S(1)} %attend.3.att_ref, bf16[2,4,8,8,32,128]{5,4,3,2,1,0:T(8,128)(2,1)S(1)} %get-tuple-element.58.wo_ref), custom_call_target="tpu_custom_call" | custom-call | tf_op jit(solution)/shard_map/cond/branch_1_fun/finish/pallas_call | solution.py:722
  148.5 0.9 copy.35
  (24 shorter events, 0.9 us)
Async XLA Ops:
  0.0 4.5 %copy-start = (bf16[1,384,2048]{2,1,0:T(8,128)(2,1)S(1)}, bf16[1,384,2048]{2,1,0:T(8,128)(2,1)}, u32[]{:S(2)}) copy-start(bf16[1,384,2048]{2,1,0:T(8,128)(2,1)} %param.12) | copy-start | bytes 4718596
  51.9 24.6 %copy-start.3 = (s32[4,4]{1,0:T(4,128)S(1)}, s32[4,4]{1,0:T(4,128)}, u32[]{:S(2)}) copy-start(s32[4,4]{1,0:T(4,128)} %lt.58) | copy-start | bytes 196

commit v3 on v2

v3 whole, which is shorter than its diff:
```python
import functools

import jax
import jax.numpy as jnp
from jax import lax
from jax.experimental import pallas as pl
from jax.experimental.pallas import tpu as pltpu
from jax.sharding import PartitionSpec as P

MESH = pl.DeviceIdType.MESH

HEADS = 16
GROUPS = 4
PER = 4
HEAD = 64
BLK = 64
PICKS = 16
N = 8
ROWS = 208
HALF = 192
SPLIT = 112
MASKED = -1e30
VMEM = pltpu.MemorySpace.VMEM
SMEM = pltpu.MemorySpace.SMEM
HBM = pltpu.MemorySpace.HBM


def place():
    kv = lax.axis_index("kv")
    return kv // N, lax.rem(kv, N)


class Copies:
    def __init__(self, send_sems, recv_sems):
        self.send_sems, self.recv_sems, self.used, self.sent = send_sems, recv_sems, 0, []

    def slot(self):
        self.used += 1
        return self.used - 1

    def send(self, i, src, dst, device):
        copy = pltpu.make_async_remote_copy(
            src_ref=src,
            dst_ref=dst,
            send_sem=self.send_sems.at[i],
            recv_sem=self.recv_sems.at[i],
            device_id=device,
            device_id_type=MESH,
        )
        copy.start()

    def arrived(self, i, ref, device):
        pltpu.make_async_remote_copy(
            src_ref=ref,
            dst_ref=ref,
            send_sem=self.send_sems.at[i],
            recv_sem=self.recv_sems.at[i],
            device_id=device,
            device_id_type=MESH,
        ).wait_recv()

    def left(self, i, ref, device):
        pltpu.make_async_remote_copy(
            src_ref=ref,
            dst_ref=ref,
            send_sem=self.send_sems.at[i],
            recv_sem=self.recv_sems.at[i],
            device_id=device,
            device_id_type=MESH,
        ).wait_send()


def when(cond, fn):
    if cond is True:
        fn()
    elif cond is not False:
        pl.when(cond)(fn)


def both(a, b):
    if a is True:
        return b
    if b is True:
        return a
    if a is False or b is False:
        return False
    return jnp.logical_and(a, b)


def wrap(i):
    return lax.rem(i + N, N)


def barrier(kinds):
    sem = pltpu.get_barrier_semaphore()
    for device in kinds:
        pl.semaphore_signal(sem, inc=1, device_id=device, device_id_type=MESH)
    pl.semaphore_wait(sem, len(kinds))


def plane_partners(z, y):
    return [{"kv": z * N + wrap(y + d)} for d in range(1, N)] + [
        {"kv": wrap(z + d) * N + y} for d in range(1, N)
    ]


class Gather:
    def __init__(
        self, copies, src, view, rows, causal, pair, parts=(True, True), tie=False, only=True
    ):
        self.c, self.src, self.view, self.rows, self.causal = copies, src, view, rows, causal
        self.pair, self.parts, self.tie = pair, parts, tie
        self.z, self.y = place()
        self.live = True if rows == N else self.z < rows
        self.only = only
        self.waits = []
        self.pair_waits = []
        self.flight = {}
        if not causal:
            self.subs_b = [(0, 4), (4, 4)]
        elif rows == N:
            self.subs_b = [(0, 1), (1, 1), (2, 2), (4, 2), (6, 2)]
        else:
            self.subs_b = [(i, 1) for i in range(rows)]

    def dev(self, z, y):
        return {"kv": z * N + y}

    def transfer(self, cond_send, src, dst, device, cond_recv, got):
        i = self.c.slot()
        cond_send, cond_recv = both(cond_send, self.only), both(cond_recv, self.only)
        when(cond_send, lambda: self.c.send(i, src, dst, device))
        self.waits.append((i, cond_send, src, device))
        return (i, cond_recv, got, device)

    def take(self, t):
        i, cond, ref, device = t
        when(cond, lambda: self.c.arrived(i, ref, device))

    def mirror(self, cond, ref):
        if self.pair is None:
            return
        i = self.c.slot()
        send, recv = cond, cond
        if self.only is not True:
            send, recv = self.only, jnp.logical_not(self.only)
        when(send, lambda: self.c.send(i, ref, ref, self.pair))
        self.pair_waits.append((i, send, recv, ref))

    def first(self):
        z, y = self.z, self.y
        self.a1, self.b1 = [], []
        for d in range(1, N) if self.parts[0] else ():
            self.a1.append(
                self.transfer(
                    self.live,
                    self.src(0),
                    self.view(z, 1, y, 1, 0),
                    self.dev(z, wrap(y + d)),
                    self.live,
                    self.view(z, 1, wrap(y - d), 1, 0),
                )
            )
        reach = N if not self.causal else self.rows
        for d in range(1, reach) if self.parts[1] else ():
            cs = True if not self.causal else z + d < self.rows
            cr = True if not self.causal else both(self.live, z - d >= 0)
            self.b1.append(
                self.transfer(
                    cs,
                    self.src(1),
                    self.view(z, 1, y, 1, 1),
                    self.dev(wrap(z + d), y),
                    cr,
                    self.view(wrap(z - d), 1, y, 1, 1),
                )
            )

    def ring_y(self, k, z0, nz, part, right, cond):
        z, y = self.z, self.y
        if right:
            o, got, to = wrap(y - (k - 1)), wrap(y - k), wrap(y + 1)
        else:
            o, got, to = lax.rem(y + k - 1, N), lax.rem(y + k, N), wrap(y - 1)
        return self.transfer(
            cond,
            self.view(z0, nz, o, 1, part),
            self.view(z0, nz, o, 1, part),
            self.dev(z, to),
            cond,
            self.view(z0, nz, got, 1, part),
        )

    def hop_a(self, right, sub, k, depth):
        z, y = self.z, self.y
        y0, ny = (sub * 4, 4)
        if right:
            o, got, to = wrap(z - (k - 1)), wrap(z - k), wrap(z + 1)
            cs = both(z - (k - 1) >= 0, z + 1 < self.rows) if self.causal else True
            cr = both(self.live, z - k >= 0) if self.causal else True
        else:
            o, got, to = wrap(z + k - 1), lax.rem(z + k, N), wrap(z - 1)
            cs = o < depth if self.causal else True
            cr = got < depth if self.causal else True
        return self.transfer(
            cs,
            self.view(o, 1, y0, ny, 0),
            self.view(o, 1, y0, ny, 0),
            self.dev(to, y),
            cr,
            self.view(got, 1, y0, ny, 0),
        )

    def hop_b(self, right, sub, k):
        z0, nz = self.subs_b[sub]
        cond = self.live
        if self.causal and z0 > 0:
            cond = both(cond, self.z >= z0)
        return self.ring_y(k, z0, nz, 1, right, cond)

    def depth_a(self, right, sub):
        if self.rows < N:
            return self.rows - 1 if right else 0
        return 4 if right == (sub == 0) else 3

    def depth_b(self, right, sub):
        return 4 if right == ((sub % 2 == 0) != self.tie) else 3

    def hop(self, k):
        steps = []
        order = [("a", 0), ("b", 0), ("b", 1), ("a", 1)] + [("b", i) for i in range(2, 5)]
        begun = set()
        for ring, s in order:
            if s >= (2 if ring == "a" else len(self.subs_b)) or not self.parts[ring == "b"]:
                continue
            if k == 1 and ring not in begun:
                begun.add(ring)
                steps.append(lambda ring=ring: self.begin(ring))
            for r in (True, False):
                steps.append(lambda ring=ring, s=s, r=r: self.lane(ring, s, r, k))
        return steps

    def begin(self, ring):
        for t in self.a1 if ring == "a" else self.b1:
            self.take(t)

    def lane(self, ring, s, r, k):
        depth = self.depth_a(r, s) if ring == "a" else self.depth_b(r, s)
        got = None
        if 1 < k <= depth + 1:
            got = self.flight[ring, r, s]
            self.take(got)
        if k <= depth:
            self.flight[ring, r, s] = (
                self.hop_a(r, s, k, depth) if ring == "a" else self.hop_b(r, s, k)
            )
        if got is not None:
            self.mirror(got[1], got[2])
        if k == 1 and r:
            if ring == "a":
                self.mirror(self.live, self.view(self.z, 1, s * 4, 4, 0))
            else:
                z0, nz = self.subs_b[s]
                cond = both(self.live, self.z >= z0) if z0 and self.causal else self.live
                self.mirror(cond, self.view(z0, nz, self.y, 1, 1))

    def last(self):
        for i, send, recv, ref in self.pair_waits:
            when(recv, lambda: self.c.arrived(i, ref, self.pair))
            when(send, lambda: self.c.left(i, ref, self.pair))
        for i, cond, ref, device in self.waits:
            when(cond, lambda: self.c.left(i, ref, device))


def spread_partners(dp, tp):
    return [{"dp": lax.rem(dp + e // 2, 4), "tp": lax.rem(tp + e % 2, 2)} for e in range(1, 8)]


def entry_kernel(
    x_ref, w_ref, o_ref, ints_ref, tok_ref, wall_ref, wo_ref, gint_ref, send_sems, recv_sems, int_sems, local_sem
):
    z, y = place()
    dp, tp = lax.axis_index("dp"), lax.axis_index("tp")
    pair = {"tp": 1 - tp}
    owner = dp // 2 == tp
    mine = x_ref.at[pl.ds(pl.multiple_of(tp * HALF, HALF), HALF)]
    local = pltpu.make_async_copy(mine, tok_ref.at[dp], local_sem)
    local.start()
    wo_ref[tp, z, y] = o_ref[...]

    @pl.when(owner)
    def _():
        wall_ref[z, y] = w_ref[...]

    barrier(plane_partners(z, y) + spread_partners(dp, tp))
    c = Copies(send_sems, recv_sems)

    left, right = lax.rem(dp + 3, 4), lax.rem(dp + 1, 4)
    part = HALF // 2
    first = {}
    for way, to, subs in (("r", right, (0, 1)), ("l", left, (1, 0))):
        for sub in subs:
            i = c.slot()
            src = x_ref.at[pl.ds(pl.multiple_of(tp * HALF + sub * part, part), part)]
            c.send(i, src, tok_ref.at[dp, pl.ds(sub * part, part)], {"dp": to})
            first[way, sub] = (i, src, to)

    def int_copy(gl, h):
        return pltpu.make_async_remote_copy(
            src_ref=ints_ref.at[gl, h],
            dst_ref=gint_ref.at[dp],
            send_sem=int_sems.at[gl * 2 + h],
            recv_sem=int_sems.at[4 + dp],
            device_id={"dp": 2 * tp + gl, "tp": jnp.int32(h)},
            device_id_type=MESH,
        )

    def is_own(gl, h):
        return jnp.logical_and(2 * tp + gl == dp, tp == h)

    for gl in range(2):
        for h in range(2):

            def go(gl=gl, h=h):
                int_copy(gl, h).start()

            def keep(gl=gl, h=h):
                gint_ref[dp] = ints_ref[gl, h]

            pl.when(jnp.logical_not(is_own(gl, h)))(go)
            pl.when(is_own(gl, h))(keep)

    jobs = []
    for src_ref, out_ref, only in ((o_ref, wo_ref.at[tp], True), (w_ref, wall_ref, owner)):
        half = src_ref.shape[0] // 2

        def src(part, src_ref=src_ref, half=half):
            return src_ref.at[pl.ds(part * half, half)]

        def view(z0, nz, y0, ny, part, out_ref=out_ref, half=half):
            zi = z0 if nz == 1 else pl.ds(z0, nz)
            yi = y0 if ny == 1 else pl.ds(y0, ny)
            return out_ref.at[zi, yi, pl.ds(part * half, half)]

        jobs.append(Gather(c, src, view, N, False, pair, only=only))
    for g in jobs:
        g.first()
    second = []

    def onward(way, sub, frm, to):
        i = first[way, sub][0]
        ref = tok_ref.at[frm, pl.ds(sub * part, part)]
        c.arrived(i, ref, {"dp": to})
        i2 = c.slot()
        c.send(i2, ref, ref, {"dp": to})
        second.append((i2, ref, sub, to))

    for k in range(1, 6):
        for g in jobs:
            for step in g.hop(k):
                step()
        if k == 2:
            onward("r", 0, left, right)
            onward("l", 1, right, left)
    assert c.used <= send_sems.shape[0], c.used
    for g in jobs:
        g.last()
    for q in range(4):

        def take(q=q):
            ref = gint_ref.at[q]
            pltpu.make_async_remote_copy(
                src_ref=ref,
                dst_ref=ref,
                send_sem=int_sems.at[0],
                recv_sem=int_sems.at[4 + q],
                device_id={"dp": jnp.int32(q), "tp": tp},
                device_id_type=MESH,
            ).wait_recv()

        pl.when(jnp.logical_not(jnp.logical_and(q == dp, owner)))(take)
    for gl in range(2):
        for h in range(2):
            pl.when(jnp.logical_not(is_own(gl, h)))(lambda gl=gl, h=h: int_copy(gl, h).wait_send())
    local.wait()
    for way, sub, frm, to in (("r", 1, left, right), ("l", 0, right, left)):
        c.arrived(first[way, sub][0], tok_ref.at[frm, pl.ds(sub * part, part)], {"dp": to})
    far = lax.rem(dp + 2, 4)
    for i2, ref, sub, to in second:
        c.arrived(i2, tok_ref.at[far, pl.ds(sub * part, part)], {"dp": to})
    for i, src, to in first.values():
        c.left(i, src, {"dp": to})
    for i2, ref, sub, to in second:
        c.left(i2, ref, {"dp": to})


def entry(x, w, o, ints):
    vm = pl.BlockSpec(memory_space=VMEM)
    return pl.pallas_call(
        entry_kernel,
        out_shape=[
            jax.ShapeDtypeStruct((4, HALF, x.shape[1]), x.dtype),
            jax.ShapeDtypeStruct((N, N) + w.shape, w.dtype),
            jax.ShapeDtypeStruct((2, N, N) + o.shape, o.dtype),
            jax.ShapeDtypeStruct((4,) + ints.shape[2:], ints.dtype),
        ],
        in_specs=[pl.BlockSpec(memory_space=HBM), vm, vm, vm],
        out_specs=[vm] * 4,
        scratch_shapes=[
            pltpu.SemaphoreType.DMA((192,)),
            pltpu.SemaphoreType.DMA((192,)),
            pltpu.SemaphoreType.DMA((8,)),
            pltpu.SemaphoreType.DMA,
        ],
        compiler_params=pltpu.CompilerParams(
            collective_id=0, has_side_effects=True, vmem_limit_bytes=24 << 20
        ),
        name="entry",
    )(x, w, o, ints)


def bases(spans):
    return [sum(spans[:r]) for r in range(4)]


def kv_kernel(spans, order_ref, got_ref, pairs_ref, out_ref, own, send_sems, recv_sems):
    z, y = place()
    tp = lax.axis_index("tp")
    pair = {"tp": 1 - tp}
    base = bases(spans)
    for r, rows in enumerate(spans):

        def fill(r=r):
            seq = order_ref[r]
            piece = got_ref[seq, :, pl.ds(PER * HEAD, 2 * HEAD)]
            pairs = pairs_ref[seq]
            for ref in (own.at[r], out_ref.at[tp, base[r] + z, y]):
                ref[pl.ds(0, HALF)] = piece
                ref[pl.ds(HALF, ROWS - HALF)] = pairs

        when(True if rows == N else z < rows, fill)
    barrier(plane_partners(z, y) + [pair])
    c = Copies(send_sems, recv_sems)
    jobs = []
    for r, rows in enumerate(spans):

        split = SPLIT if r == 0 else 0

        def part_rows(part, split=split):
            return pl.ds(0, split) if part == 0 else pl.ds(split, ROWS - split)

        def src(part, r=r, part_rows=part_rows):
            return own.at[r, part_rows(part)]

        def view(z0, nz, y0, ny, part, r=r, part_rows=part_rows):
            zi = base[r] + z0 if nz == 1 else pl.ds(base[r] + z0, nz)
            yi = y0 if ny == 1 else pl.ds(y0, ny)
            return out_ref.at[tp, zi, yi, part_rows(part)]

        jobs.append(Gather(c, src, view, rows, True, pair, (r == 0, True), r % 2 == 1))
    for g in jobs:
        g.first()
    for k in range(1, 6):
        for g in jobs:
            for step in g.hop(k):
                step()
    assert c.used <= send_sems.shape[0], c.used
    for g in jobs:
        g.last()


def gather_kv(order, got, pairs, spans, number, limit):
    vm = pl.BlockSpec(memory_space=VMEM)
    return pl.pallas_call(
        functools.partial(kv_kernel, spans),
        out_shape=jax.ShapeDtypeStruct((2, sum(spans), N, ROWS, 2 * HEAD), got.dtype),
        in_specs=[pl.BlockSpec(memory_space=SMEM), vm, vm],
        out_specs=vm,
        scratch_shapes=[
            pltpu.VMEM((4, ROWS, 2 * HEAD), jnp.bfloat16),
            pltpu.SemaphoreType.DMA((limit,)),
            pltpu.SemaphoreType.DMA((limit,)),
        ],
        compiler_params=pltpu.CompilerParams(
            collective_id=number,
            has_side_effects=True,
            vmem_limit_bytes=(24 if sum(spans) < 20 else 40) << 20,
        ),
        name="gather_kv",
    )(order, got, pairs)


def attend_kernel(
    spans, order_ref, ints_ref, main_ref, gate_ref, kv_ref, block_ref, out_ref, buf, comp
):
    kv, tp = lax.axis_index("kv"), lax.axis_index("tp")
    start = kv * (2 * HALF) + tp * HALF
    base = bases(spans)
    lane = lax.broadcasted_iota(jnp.int32, (BLK, 128), 1)
    row_in = lax.rem(lax.broadcasted_iota(jnp.int32, (PER * BLK, 1), 0), BLK)
    comp[...] = jnp.zeros_like(comp)
    to_row = lax.broadcasted_iota(jnp.int32, (48, 256), 0)
    from_row = lax.broadcasted_iota(jnp.int32, (48, 256), 1)
    piece = (to_row * 21846) >> 16
    pick_rows = jnp.where(from_row == piece * 16 + (to_row - piece * 3), 1.0, 0.0).astype(jnp.bfloat16)
    block_ends = block_ref[...] * BLK + (BLK - 1)

    def step(n, carry):
        r = (n * 21846) >> 16
        j = n - r * 3
        seq = order_ref[r]
        rows = pl.ds(pl.multiple_of(j * BLK, BLK), BLK)
        live = start < ints_ref[seq, 7, 0]
        first = jnp.int32(base[0])
        for q in range(1, 4):
            first = jnp.where(r == q, base[q], first)

        @pl.when(jnp.logical_and(live, j == 0))
        def _():
            def pack(zs):
                for z in zs:
                    at = jnp.minimum(first + z, sum(spans) - 1)
                    tile = kv_ref[:, at, :, pl.ds(HALF, 16), :].reshape(256, 128)
                    got = jnp.dot(pick_rows, tile, preferred_element_type=jnp.float32)
                    got = jnp.where(z <= kv // N, got, 0.0)
                    comp[pl.ds(z * 48, 48), :] = got.astype(jnp.bfloat16)

            pack((0, 1))
            pl.when(kv >= 2 * N)(lambda: pack((2, 3)))
            pl.when(kv >= 4 * N)(lambda: pack((4, 5, 6, 7)))

        @pl.when(jnp.logical_not(live))
        def _():
            out_ref[seq, rows] = jnp.zeros((BLK, PER * HEAD), jnp.bfloat16)

        @pl.when(live)
        def _():
            def fetch(p, count):
                b = ints_ref[seq, j, p]

                @pl.when(b >= 0)
                def _():
                    span = (b * 10923) >> 16
                    at = b - span * 6
                    t = jnp.where(at >= 3, 1, 0)
                    row = (at - t * 3) * BLK
                    buf[pl.ds(pl.multiple_of(count * BLK, BLK), BLK), :] = kv_ref[
                        t,
                        first + (span >> 3),
                        span & 7,
                        pl.ds(pl.multiple_of(row, BLK), BLK),
                        :,
                    ]

                return count + jnp.where(b >= 0, 1, 0)

            count = lax.fori_loop(0, PICKS, fetch, jnp.int32(0), unroll=True)
            parts = []
            for h in range(PER):
                two = main_ref[seq, rows, pl.ds((h // 2) * 128, 128)].astype(jnp.float32) * 0.125
                if h % 2:
                    two = pltpu.roll(two, 64, 1)
                parts.append(jnp.where(lane < HEAD, two, 0.0).astype(jnp.bfloat16))
            q = jnp.concatenate(parts, axis=0)

            def score(keys):
                return lax.dot_general(
                    q, keys, (((1,), (1,)), ((), ())), preferred_element_type=jnp.float32
                )

            spot = start + j * BLK + row_in
            own = main_ref[seq, rows, pl.ds(PER * HEAD, 128)]
            ks = lax.broadcasted_iota(jnp.int32, (1, BLK), 1)

            def run(most, far_too):
                keys = comp[pl.ds(0, most), :]
                cs = jnp.where(block_ends[:, :most] <= spot, score(keys), MASKED)
                ctop = jnp.max(cs, axis=-1, keepdims=True)
                cw = jnp.exp(cs - ctop)
                cn = jnp.maximum(jnp.sum(cw, axis=-1, keepdims=True), 1.0)
                cp = (cw * jnp.where(spot >= BLK - 1, 1.0 / cn, 0.0)).astype(jnp.bfloat16)
                co = jnp.dot(cp, keys, preferred_element_type=jnp.float32)

                os = jnp.where(ks <= row_in, score(own), MASKED)
                top = jnp.max(os, axis=-1, keepdims=True)
                if far_too:
                    far = buf[...]
                    spots = lax.broadcasted_iota(jnp.int32, (1, PICKS * BLK), 1)
                    fs = jnp.where(spots < count * BLK, score(far), MASKED)
                    top = jnp.maximum(top, jnp.max(fs, axis=-1, keepdims=True))
                ow = jnp.exp(os - top)
                total = jnp.sum(ow, axis=-1, keepdims=True)
                if far_too:
                    fw = jnp.exp(fs - top)
                    total = total + jnp.sum(fw, axis=-1, keepdims=True)
                inv = 1.0 / total
                so = jnp.dot((ow * inv).astype(jnp.bfloat16), own, preferred_element_type=jnp.float32)
                if far_too:
                    so = so + jnp.dot(
                        (fw * inv).astype(jnp.bfloat16), far, preferred_element_type=jnp.float32
                    )
                mixed = []
                g = gate_ref[seq, rows]
                for h in range(PER):
                    at = slice(h * BLK, (h + 1) * BLK)
                    mixed.append(g[:, h : h + 1] * co[at] + g[:, 4 + h : 5 + h] * so[at])
                for h in range(2):
                    pair = jnp.where(
                        lane < HEAD, pltpu.roll(mixed[2 * h], 64, 1), mixed[2 * h + 1]
                    )
                    out_ref[seq, rows, pl.ds(h * 128, 128)] = pair.astype(jnp.bfloat16)

            low, some = kv < 2 * N, count > 0
            for cond_low, most in ((low, 128), (jnp.logical_not(low), 384)):
                for cond_far, far_too in ((some, True), (jnp.logical_not(some), False)):
                    pl.when(jnp.logical_and(cond_low, cond_far))(
                        functools.partial(run, most, far_too)
                    )

        return carry

    buf[...] = jnp.zeros_like(buf)
    lax.fori_loop(0, 12, step, 0)


def attend(spans, order, gint, got, gates, gathered):
    vm = pl.BlockSpec(memory_space=VMEM)
    sm = pl.BlockSpec(memory_space=SMEM)
    c = jnp.arange(384, dtype=jnp.int32)
    z, t, y, j = c // 48, c % 48 // 24, c % 24 // 3, c % 3
    blocks = ((z * N + y) * 6 + t * 3 + j)[None]
    return pl.pallas_call(
        functools.partial(attend_kernel, spans),
        out_shape=jax.ShapeDtypeStruct((4, HALF, PER * HEAD), jnp.bfloat16),
        in_specs=[sm, sm, vm, vm, vm, vm],
        out_specs=vm,
        scratch_shapes=[
            pltpu.VMEM((PICKS * BLK, 2 * HEAD), jnp.bfloat16),
            pltpu.VMEM((384, 2 * HEAD), jnp.bfloat16),
        ],
        compiler_params=pltpu.CompilerParams(vmem_limit_bytes=(24 if sum(spans) < 20 else 48) << 20),
        name="attend",
    )(order, gint, got, gates, gathered, blocks)


def finish_kernel(len_ref, att_ref, wo_ref, out_ref, back, send_sems, recv_sems):
    dp, kv, tp = lax.axis_index("dp"), lax.axis_index("kv"), lax.axis_index("tp")
    barrier([{"dp": lax.rem(dp + d, 4)} for d in range(1, 4)])

    def copy(d):
        to = lax.rem(dp + d, 4)
        return pltpu.make_async_remote_copy(
            src_ref=att_ref.at[to],
            dst_ref=back.at[dp],
            send_sem=send_sems.at[d],
            recv_sem=recv_sems.at[d],
            device_id={"dp": to},
            device_id_type=MESH,
        )

    for d in (2, 1, 3):
        copy(d).start()
    back[dp] = att_ref[dp]

    def arrived(frm):
        d = lax.rem(dp + 4 - frm, 4)
        pltpu.make_async_remote_copy(
            src_ref=back.at[frm],
            dst_ref=back.at[frm],
            send_sem=send_sems.at[d],
            recv_sem=recv_sems.at[d],
            device_id={"dp": frm},
            device_id_type=MESH,
        ).wait_recv()

    spot = kv * (2 * HALF) + tp * HALF + lax.broadcasted_iota(jnp.int32, (HALF, 1), 0)
    alive = spot < len_ref[0]

    def tiles(t, last):
        cols = jnp.concatenate([back[2 * t], back[2 * t + 1]], axis=1)

        def tile(z, carry):
            w = wo_ref[t, z].reshape(256, 512)
            part = lax.dot_general(
                cols, w, (((1,), (1,)), ((), ())), preferred_element_type=jnp.float32
            ).astype(jnp.bfloat16)
            at = pl.ds(pl.multiple_of(z * 256, 256), 256)
            if last:
                both_sets = out_ref[:, at].astype(jnp.float32) + part.astype(jnp.float32)
                part = jnp.where(alive, both_sets, 0.0).astype(jnp.bfloat16)
            out_ref[:, at] = part
            return carry

        lax.fori_loop(0, N, tile, 0, unroll=2)

    near = dp // 2
    arrived(4 * near + 1 - dp)
    tiles(near, False)
    arrived(2 - 2 * near)
    arrived(3 - 2 * near)
    tiles(1 - near, True)
    for d in (1, 2, 3):
        copy(d).wait_send()


def finish(length, att, wo, number):
    vm = pl.BlockSpec(memory_space=VMEM)
    return pl.pallas_call(
        finish_kernel,
        out_shape=jax.ShapeDtypeStruct((HALF, 2048), jnp.bfloat16),
        in_specs=[pl.BlockSpec(memory_space=SMEM), vm, vm],
        out_specs=vm,
        scratch_shapes=[
            pltpu.VMEM((4, HALF, PER * HEAD), jnp.bfloat16),
            pltpu.SemaphoreType.DMA((4,)),
            pltpu.SemaphoreType.DMA((4,)),
        ],
        compiler_params=pltpu.CompilerParams(
            collective_id=number, has_side_effects=True, vmem_limit_bytes=24 << 20
        ),
        name="finish",
    )(length, att, wo)


def body(
    tokens, seq_lengths, block_picks, w_query, w_key, w_value, w_gate, w_ckey, w_cvalue, w_out
):
    x = tokens[0]
    dp = lax.axis_index("dp")
    low = lax.rem(dp, 2) == 0
    piece = jnp.where(
        low,
        jnp.concatenate([w_query[:, :256], w_key[:, :64], w_value[:, :64]], axis=1),
        jnp.concatenate([w_query[:, 256:], w_key[:, 64:], w_value[:, 64:]], axis=1),
    )
    picks = block_picks[0].transpose(1, 0, 2).reshape(2, 2, 3, PICKS)
    ints = jnp.pad(picks, ((0, 0), (0, 0), (0, 5), (0, 112)))
    row = lax.broadcasted_iota(jnp.int32, ints.shape, 2)
    ints = jnp.where(row == 7, seq_lengths[0], ints)
    toks, w_all, wo, gint = entry(x, piece, w_out.T, ints)
    toks = toks.reshape(4 * HALF, 2048)

    gate_cols = lax.dynamic_index_in_dim(w_gate.reshape(2048, 2, GROUPS, PER), dp, 2, keepdims=False)
    gates = jax.nn.sigmoid(
        jnp.dot(toks, gate_cols.reshape(2048, 8), preferred_element_type=jnp.float32)
    ).reshape(4, HALF, 8)
    qkv = jnp.dot(toks, w_all.reshape(2048, 384), preferred_element_type=jnp.float32)
    qkv = qkv.astype(jnp.bfloat16)
    flat = qkv.reshape(12, BLK, 384)
    ck = jnp.dot(
        flat[..., 256:320].reshape(12, BLK * HEAD), w_ckey, preferred_element_type=jnp.float32
    )
    cv = jnp.dot(
        flat[..., 320:].reshape(12, BLK * HEAD), w_cvalue, preferred_element_type=jnp.float32
    )
    pairs = jnp.concatenate([ck, cv], axis=1).astype(jnp.bfloat16).reshape(4, 3, 128)
    pairs = jnp.pad(pairs, ((0, 0), (0, 13), (0, 0)))
    got = qkv.reshape(4, HALF, 384)
    lens = gint[:, 7, 0]
    ids = jnp.arange(4, dtype=jnp.int32)
    ahead = (lens[None, :] > lens[:, None]) | (
        (lens[None, :] == lens[:, None]) & (ids[None, :] < ids[:, None])
    )
    rank = jnp.sum(ahead.astype(jnp.int32), axis=1)
    order = jnp.sum(jnp.where(rank[None, :] == ids[:, None], ids[None, :], 0), axis=1)
    ranked = jnp.sum(
        jnp.where(rank[None, :] == ids[:, None], lens[None, :], 0), axis=1
    )

    def run(spans, number, limit):
        gathered = gather_kv(order, got, pairs, spans, number, limit)
        att = attend(spans, order, gint, got, gates, gathered)
        return finish(seq_lengths, att, wo, number + 1)

    span = N * 384
    small = (ranked[1] <= 3 * span) & (ranked[2] <= 2 * span) & (ranked[3] <= span)
    out = lax.cond(
        small, lambda: run((8, 3, 2, 1), 2, 448), lambda: run((8, 8, 8, 8), 4, 600)
    )
    return out[None]


def solution(mesh):
    return jax.shard_map(
        body,
        mesh=mesh,
        in_specs=(
            P("dp", "kv", None),
            P("dp"),
            P("dp", "kv", "tp", None),
            P("kv", "tp"),
            P("kv", "tp"),
            P("kv", "tp"),
            P(),
            P(),
            P(),
            P("tp", "kv"),
        ),
        out_specs=P("dp", ("kv", "tp"), None),
        check_vma=False,
    )
```

time: 150 us -> 131 us (0.87)
  Pallas kernels: 130 us -> 116 us
  matrix products: 8.52 us -> 3.25 us
    pallas_call x3 -> x2, Pallas kernels: 99.9 us -> 88.4 us  [the longest x1 46.9 us: entry(): pl.pallas_call(entry_kernel, out_shape=[jax.ShapeDtypeStruct((4, HALF, x....]
    dot_general x6 -> x4, matrix products: 8.52 us -> 3.25 us  [the longest x1 1.8 us: body(): jnp.dot(toks, w_all.reshape(2048, 384), preferred_element_type=jnp.float32)]
    pallas_call x1, Pallas kernels: 17.7 us -> 15.5 us  [attend(): pl.pallas_call(functools.partial(attend_kernel, spans), out_shape=jax.Sha...]
    unnamed x5 -> x9, local copies, waits for them, and re-layouts: 0.89 us -> 3.05 us
where the time goes in v3:
time: 131 us
  Pallas kernels  116 us (89%)
  local copies, waits for them, and re-layouts  7.85 us (6%)
  matrix products  3.25 us (2%)
  between operations  2.75 us (2%)
    pallas_call x1, Pallas kernels, entry(): pl.pallas_call(entry_kernel, out_shape=[jax.ShapeDtypeStruct((4, HALF, x....  46.9 us
    pallas_call x1, Pallas kernels, gather_kv(): pl.pallas_call(functools.partial(kv_kernel, spans), out_shape=jax.ShapeDt...  41.5 us
    pallas_call x1, Pallas kernels, attend(): pl.pallas_call(functools.partial(attend_kernel, spans), out_shape=jax.Sha...  15.5 us
    pallas_call x1, Pallas kernels, finish(): pl.pallas_call(finish_kernel, out_shape=jax.ShapeDtypeStruct((HALF, 2048)...  12 us
    unnamed x9, local copies, waits for them, and re-layouts  3.05 us

profile of v3, /device:TPU:1, one launch (start us, length us, event | category | flops | bytes accessed | tf_op | source)
XLA Modules:
  0.0 130.7 jit_solution(12528282177948691526)
XLA Ops:
  0.0 0.0 copy-start
  0.7 0.7 copy.20
  1.4 0.1 pad_select_fusion.ints_ref
  1.5 0.9 fusion.18
  2.4 0.7 fusion.17
  3.1 0.1 maximum_select_fusion.w_ref
  3.2 1.0 reshape.370
  4.2 0.0 copy-start.1
  4.2 1.4 %copy-done.1 = bf16[1,384,2048]{2,1,0:T(8,128)(2,1)S(1)} copy-done((bf16[1,384,2048]{2,1,0:T(8,128)(2,1)S(1)}, bf16[1,384,2048]{2,1,0:T(8,128)(2,1)}, u32[]{:S(2)}) %copy-start.1) | copy-done | bytes 1572888
  5.6 0.8 copy-done.2
  6.4 46.9 %entry.1 = (bf16[4,192,2048]{2,1,0:T(8,128)(2,1)S(1)}, bf16[8,8,32,384]{3,2,1,0:T(8,128)(2,1)S(1)}, bf16[2,8,8,32,512]{4,3,2,1,0:T(8,128)(2,1)}, s32[4,8,128]{2,1,0:T(8,128)S(1)}) custom-call(bf16[384,2048]{1,0:T(8,128)(2,1)S(1)} %bitcast.39, bf16[32,384]{1,0:T(8,128)(2,1)S(1)} %maximum_select_fusion.w_ref, bf16[32,512]{1,0:T(8,128)(2,1)S(1)} %bitcast.40, ...), custom_call_target="tpu_custom_call" | custom-call | tf_op jit(solution)/shard_map/entry/pallas_call | solution.py:399
  53.3 0.9 fusion.21
  54.2 1.8 %convolution_convert_fusion = bf16[768,384]{1,0:T(8,128)(2,1)S(1)} fusion(bf16[768,2048]{1,0:T(8,128)(2,1)S(1)} %bitcast.36, bf16[2048,384]{1,0:T(8,128)(2,1)S(1)} %bitcast.41), kind=kOutput, calls=%fused_computation.36 | convolution fusion | flops 1208254464 | bytes 5308416 | tf_op jit(solution)/shard_map/dot_general | solution.py:747
  56.0 0.2 slice_reduce_fusion
  56.2 0.2 convert_reduce_fusion
  56.3 0.1 select_reduce_fusion.2
  56.5 0.7 fusion.20
  59.1 0.1 fusion.16
  59.2 0.2 dot_general.18
  59.4 0.0 copy-done
  59.4 0.3 fusion.12
  59.7 0.2 dot_general.20
  59.9 0.3 fusion.10
  60.2 0.1 pad_maximum_fusion
  60.2 69.6 %conditional.1 = (bf16[1,192,2048]{2,1,0:T(8,128)(2,1)S(1)}) conditional(s32[]{:T(128)} %bitcast.6, (pred[4,4]{1,0:T(4,128)(4,1)S(1)}, s32[4,4]{1,0:T(4,128)S(1)}, s32[4,4]{1,0:T(4,128)S(1)}, bf16[768,384]{1,0:T(8,128)(2,1)S(1)}, f32[768,8]{0,1:T(8,128)S(1)}, /*index=5*/bf16[4,3,128]{2,0,1:T(4,128)(2,1)S(1)}, s32[4,8,128]{2,1,0:T(8,128)S(1)}, ...), branch_computations={%region_2.4_spmd.clone, %region_4.6_spmd.clone} | conditional | flops 36124 | bytes 16902854 | solution.py:777
  60.4 0.1 select_reduce_fusion.1.order_ref
  60.6 0.2 copy.25
  60.7 0.1 add_divide_fusion.1
  60.9 41.5 %gather_kv.3.kv_ref = bf16[2,14,8,208,128]{4,3,2,1,0:T(8,128)(2,1)S(1)} custom-call(s32[4]{0:T(128)S(1)} %select_reduce_fusion.1.order_ref, bf16[4,192,384]{2,1,0:T(8,128)(2,1)S(1)} %bitcast.45, bf16[4,16,128]{2,1,0:T(8,128)(2,1)S(1)} %pad.16.pairs_ref), custom_call_target="tpu_custom_call" | custom-call | tf_op jit(solution)/shard_map/cond/branch_1_fun/gather_kv/pallas_call | solution.py:474
  102.3 15.5 %attend.3.att_ref = bf16[4,192,256]{2,1,0:T(8,128)(2,1)S(1)} custom-call(s32[4]{0:T(128)S(1)} %select_reduce_fusion.1.order_ref, s32[4,8,128]{2,1,0:T(8,128)S(1)} %get-tuple-element.170.ints_ref, bf16[4,192,384]{2,1,0:T(8,128)(2,1)S(1)} %bitcast.46, f32[4,192,8]{2,1,0:T(8,128)S(1)} %bitcast.38, bf16[2,14,8,208,128]{4,3,2,1,0:T(8,128)(2,1)S(1)} %gather_kv.3.kv_ref, ...), custom_call_target="tpu_custom_call" | custom-call | tf_op jit(solution)/shard_map/cond/branch_1_fun/attend/pallas_call | solution.py:632
  117.9 12.0 %finish.5 = bf16[192,2048]{1,0:T(8,128)(2,1)S(1)} custom-call(s32[1]{0:T(128)} %get-tuple-element.166.len_ref, bf16[4,192,256]{2,1,0:T(8,128)(2,1)S(1)} %attend.3.att_ref, bf16[2,8,8,32,512]{4,3,2,1,0:T(8,128)(2,1)S(1)} %copy-done.4), custom_call_target="tpu_custom_call" | custom-call | tf_op jit(solution)/shard_map/cond/branch_1_fun/finish/pallas_call | solution.py:708
  129.9 0.9 copy.39
  (16 shorter events, 0.1 us)
Async XLA Ops:
  0.0 59.4 %copy-start = (bf16[4096,64]{0,1:T(8,128)(2,1)S(1)}, bf16[4096,64]{0,1:T(8,128)(2,1)}, u32[]{:S(2)}) copy-start(bf16[4096,64]{0,1:T(8,128)(2,1)} %param.19) | copy-start | bytes 1572868
  4.2 1.4 %copy-start.1 = (bf16[1,384,2048]{2,1,0:T(8,128)(2,1)S(1)}, bf16[1,384,2048]{2,1,0:T(8,128)(2,1)}, u32[]{:S(2)}) copy-start(bf16[1,384,2048]{2,1,0:T(8,128)(2,1)} %param.12) | copy-start | bytes 4718596
  5.6 0.8 copy-start.2
  54.2 5.7 %copy-start.5 = (bf16[4096,64]{0,1:T(8,128)(2,1)S(1)}, bf16[4096,64]{0,1:T(8,128)(2,1)}, u32[]{:S(2)}) copy-start(bf16[4096,64]{0,1:T(8,128)(2,1)} %param.20) | copy-start | bytes 1572868
  102.3 15.5 %copy-start.4 = (bf16[2,8,8,32,512]{4,3,2,1,0:T(8,128)(2,1)S(1)}, bf16[2,8,8,32,512]{4,3,2,1,0:T(8,128)(2,1)}, u32[]{:S(2)}) copy-start(bf16[2,8,8,32,512]{4,3,2,1,0:T(8,128)(2,1)} %get-tuple-element.174.wo_ref) | copy-start | bytes 12582916 | tf_op jit(solution)/shard_map/cond

commit v4 on v3

--- a/solution.py
+++ b/solution.py
@@ -277,7 +277,24 @@
 
 
 def entry_kernel(
-    x_ref, w_ref, o_ref, ints_ref, tok_ref, wall_ref, wo_ref, gint_ref, send_sems, recv_sems, int_sems, local_sem
+    x_ref,
+    w_ref,
+    o_ref,
+    ints_ref,
+    wg_ref,
+    qkv_ref,
+    gate_ref,
+    wo_ref,
+    gint_ref,
+    tok_ref,
+    wall_ref,
+    wcat_ref,
+    wg_buf,
+    send_sems,
+    recv_sems,
+    int_sems,
+    local_sem,
+    gate_sem,
 ):
     z, y = place()
     dp, tp = lax.axis_index("dp"), lax.axis_index("tp")
@@ -286,6 +303,8 @@
     mine = x_ref.at[pl.ds(pl.multiple_of(tp * HALF, HALF), HALF)]
     local = pltpu.make_async_copy(mine, tok_ref.at[dp], local_sem)
     local.start()
+    gate_copy = pltpu.make_async_copy(wg_ref, wg_buf, gate_sem)
+    gate_copy.start()
     wo_ref[tp, z, y] = o_ref[...]
 
     @pl.when(owner)
@@ -365,6 +384,28 @@
     assert c.used <= send_sems.shape[0], c.used
     for g in jobs:
         g.last()
+
+    frm_col = lax.broadcasted_iota(jnp.int32, (2 * HEADS, 128), 0)
+    to_col = lax.broadcasted_iota(jnp.int32, (2 * HEADS, 128), 1)
+    wanted = (to_col >> 2) * HEADS + dp * PER + (to_col & 3)
+    chosen = jnp.logical_and(frm_col == wanted, to_col < 8)
+    gate_copy.wait()
+    width = wall_ref.shape[3]
+    wcat_ref[:, pl.ds(0, width)] = wall_ref[...].reshape(wcat_ref.shape[0], width)
+    wcat_ref[:, pl.ds(width, 128)] = lax.dot_general(
+        wg_buf[...],
+        jnp.where(chosen, 1.0, 0.0).astype(jnp.bfloat16),
+        (((0,), (0,)), ((), ())),
+        preferred_element_type=jnp.float32,
+    ).astype(jnp.bfloat16)
+
+    def project(q):
+        got = jnp.dot(tok_ref[q], wcat_ref[...], preferred_element_type=jnp.float32)
+        qkv_ref[q] = got[:, :width].astype(jnp.bfloat16)
+        gate_ref[q] = lax.logistic(got[:, width : width + 16])
+
+    local.wait()
+    project(dp)
     for q in range(4):
 
         def take(q=q):
@@ -382,41 +423,51 @@
     for gl in range(2):
         for h in range(2):
             pl.when(jnp.logical_not(is_own(gl, h)))(lambda gl=gl, h=h: int_copy(gl, h).wait_send())
-    local.wait()
     for way, sub, frm, to in (("r", 1, left, right), ("l", 0, right, left)):
         c.arrived(first[way, sub][0], tok_ref.at[frm, pl.ds(sub * part, part)], {"dp": to})
+        project(frm)
     far = lax.rem(dp + 2, 4)
     for i2, ref, sub, to in second:
         c.arrived(i2, tok_ref.at[far, pl.ds(sub * part, part)], {"dp": to})
+    project(far)
     for i, src, to in first.values():
         c.left(i, src, {"dp": to})
     for i2, ref, sub, to in second:
         c.left(i2, ref, {"dp": to})
 
 
-def entry(x, w, o, ints):
+def entry(x, w, o, ints, wg):
     vm = pl.BlockSpec(memory_space=VMEM)
+    hbm = pl.BlockSpec(memory_space=HBM)
     return pl.pallas_call(
         entry_kernel,
         out_shape=[
-            jax.ShapeDtypeStruct((4, HALF, x.shape[1]), x.dtype),
-            jax.ShapeDtypeStruct((N, N) + w.shape, w.dtype),
+            jax.ShapeDtypeStruct((4, HALF, w.shape[1]), x.dtype),
+            jax.ShapeDtypeStruct((4, HALF, 16), jnp.float32),
             jax.ShapeDtypeStruct((2, N, N) + o.shape, o.dtype),
             jax.ShapeDtypeStruct((4,) + ints.shape[2:], ints.dtype),
         ],
-        in_specs=[pl.BlockSpec(memory_space=HBM), vm, vm, vm],
+        in_specs=[hbm, vm, vm, vm, hbm],
         out_specs=[vm] * 4,
         scratch_shapes=[
+            pltpu.VMEM((4, HALF, x.shape[1]), x.dtype),
+            pltpu.VMEM((N, N) + w.shape, w.dtype),
+            pltpu.VMEM((x.shape[1], w.shape[1] + 128), w.dtype),
+            pltpu.VMEM(wg.shape, wg.dtype),
             pltpu.SemaphoreType.DMA((192,)),
             pltpu.SemaphoreType.DMA((192,)),
             pltpu.SemaphoreType.DMA((8,)),
             pltpu.SemaphoreType.DMA,
+            pltpu.SemaphoreType.DMA,
         ],
         compiler_params=pltpu.CompilerParams(
-            collective_id=0, has_side_effects=True, vmem_limit_bytes=24 << 20
+            collective_id=0, has_side_effects=True, vmem_limit_bytes=60 << 20
+        ),
+        cost_estimate=pl.CostEstimate(
+            flops=30_000_000_000, bytes_accessed=8 << 20, transcendentals=0
         ),
         name="entry",
-    )(x, w, o, ints)
+    )(x, w, o, ints, wg)
 
 
 def bases(spans):
@@ -486,6 +537,9 @@
             has_side_effects=True,
             vmem_limit_bytes=(24 if sum(spans) < 20 else 40) << 20,
         ),
+        cost_estimate=pl.CostEstimate(
+            flops=30_000_000_000, bytes_accessed=8 << 20, transcendentals=0
+        ),
         name="gather_kv",
     )(order, got, pairs)
 
@@ -554,7 +608,12 @@
 
                 return count + jnp.where(b >= 0, 1, 0)
 
-            count = lax.fori_loop(0, PICKS, fetch, jnp.int32(0), unroll=True)
+            count = ints_ref[seq, j, PICKS]
+
+            @pl.when(count > 0)
+            def _():
+                lax.fori_loop(0, PICKS, fetch, jnp.int32(0), unroll=True)
+
             parts = []
             for h in range(PER):
                 two = main_ref[seq, rows, pl.ds((h // 2) * 128, 128)].astype(jnp.float32) * 0.125
@@ -734,18 +793,15 @@
         jnp.concatenate([w_query[:, 256:], w_key[:, 64:], w_value[:, 64:]], axis=1),
     )
     picks = block_picks[0].transpose(1, 0, 2).reshape(2, 2, 3, PICKS)
+    valid = jnp.sum((picks >= 0).astype(jnp.int32), axis=3, keepdims=True)
     ints = jnp.pad(picks, ((0, 0), (0, 0), (0, 5), (0, 112)))
+    valid = jnp.pad(valid, ((0, 0), (0, 0), (0, 5), (0, 0)))
     row = lax.broadcasted_iota(jnp.int32, ints.shape, 2)
-    ints = jnp.where(row == 7, seq_lengths[0], ints)
-    toks, w_all, wo, gint = entry(x, piece, w_out.T, ints)
-    toks = toks.reshape(4 * HALF, 2048)
-
-    gate_cols = lax.dynamic_index_in_dim(w_gate.reshape(2048, 2, GROUPS, PER), dp, 2, keepdims=False)
-    gates = jax.nn.sigmoid(
-        jnp.dot(toks, gate_cols.reshape(2048, 8), preferred_element_type=jnp.float32)
-    ).reshape(4, HALF, 8)
-    qkv = jnp.dot(toks, w_all.reshape(2048, 384), preferred_element_type=jnp.float32)
-    qkv = qkv.astype(jnp.bfloat16)
+    col = lax.broadcasted_iota(jnp.int32, ints.shape, 3)
+    ints = jnp.where(row == 7, seq_lengths[0], jnp.where(col == PICKS, valid, ints))
+    got, gates, wo, gint = entry(x, piece, w_out.T, ints, w_gate.T)
+
+    qkv = got.reshape(4 * HALF, 384)
     flat = qkv.reshape(12, BLK, 384)
     ck = jnp.dot(
         flat[..., 256:320].reshape(12, BLK * HEAD), w_ckey, preferred_element_type=jnp.float32
@@ -755,7 +811,6 @@
     )
     pairs = jnp.concatenate([ck, cv], axis=1).astype(jnp.bfloat16).reshape(4, 3, 128)
     pairs = jnp.pad(pairs, ((0, 0), (0, 13), (0, 0)))
-    got = qkv.reshape(4, HALF, 384)
     lens = gint[:, 7, 0]
     ids = jnp.arange(4, dtype=jnp.int32)
     ahead = (lens[None, :] > lens[:, None]) | (

time: 131 us -> 129 us (0.985)
  local copies, waits for them, and re-layouts: 7.85 us -> 4.7 us
  matrix products: 3.25 us -> 0.53 us
  Pallas kernels: 116 us -> 118 us
  other arithmetic: 0.82 us -> 2.78 us
    pallas_call x1, Pallas kernels: 46.9 us -> 50.4 us  [entry(): pl.pallas_call(entry_kernel, out_shape=[jax.ShapeDtypeStruct((4, HALF, w....]
    dot_general x2 -> x0, matrix products: 2.71 us -> none  [the longest x1 1.8 us: body(): jnp.dot(toks, w_all.reshape(2048, 384), preferred_element_type=jnp.float32)]
    unnamed x9 -> x5, local copies, waits for them, and re-layouts: 3.05 us -> 0.89 us
    pallas_call x1, Pallas kernels: 15.5 us -> 13.8 us  [attend(): pl.pallas_call(functools.partial(attend_kernel, spans), out_shape=jax.Sha...]
where the time goes in v4:
time: 129 us
  Pallas kernels  118 us (91%)
  local copies, waits for them, and re-layouts  4.7 us (4%)
  other arithmetic  2.78 us (2%)
  between operations  2.72 us (2%)
    pallas_call x1, Pallas kernels, entry(): pl.pallas_call(entry_kernel, out_shape=[jax.ShapeDtypeStruct((4, HALF, w....  50.4 us
    pallas_call x1, Pallas kernels, gather_kv(): pl.pallas_call(functools.partial(kv_kernel, spans), out_shape=jax.ShapeDt...  41.8 us
    pallas_call x1, Pallas kernels, attend(): pl.pallas_call(functools.partial(attend_kernel, spans), out_shape=jax.Sha...  13.8 us
    pallas_call x1, Pallas kernels, finish(): pl.pallas_call(finish_kernel, out_shape=jax.ShapeDtypeStruct((HALF, 2048)...  11.9 us

profile of v4, /device:TPU:1, one launch (start us, length us, event | category | flops | bytes accessed | tf_op | source)
XLA Modules:
  0.0 128.9 jit_solution(17521744254532553850)
XLA Ops:
  0.0 0.0 copy-start
  0.7 0.9 fusion.12
  1.6 0.1 copy.21
  1.7 0.1 broadcast_in_dim.50
  1.8 0.7 copy.22
  2.5 0.7 select_select_fusion.ints_ref
  3.2 0.9 fusion.17
  4.0 0.7 fusion.16
  4.8 0.7 maximum_select_fusion.w_ref
  5.5 0.0 copy-start.3
  5.5 50.4 %entry.1 = (bf16[4,192,384]{2,1,0:T(8,128)(2,1)S(1)}, f32[4,192,16]{2,1,0:T(8,128)S(1)}, bf16[2,8,8,32,512]{4,3,2,1,0:T(8,128)(2,1)}, s32[4,8,128]{2,1,0:T(8,128)S(1)}) custom-call(bf16[384,2048]{1,0:T(8,128)(2,1)} %bitcast.29, bf16[32,384]{1,0:T(8,128)(2,1)} %maximum_select_fusion.w_ref, bf16[32,512]{1,0:T(8,128)(2,1)} %bitcast.31, ...), custom_call_target="tpu_custom_call" | custom-call | flops 30000001024 | bytes 8388608 | tf_op jit(solution)/shard_map/entry/pallas_call | solution.py:442
  55.9 0.2 slice_reduce_fusion
  56.1 0.2 convert_reduce_fusion
  56.3 0.1 select_reduce_fusion.2
  56.4 0.7 fusion.19
  59.0 0.1 fusion.15
  59.1 0.2 dot_general.10
  59.3 0.0 copy-done
  59.3 0.3 convolution_convert_fusion.1
  59.6 0.2 dot_general.12
  59.7 0.0 copy-done.3
  59.8 0.3 convolution_convert_fusion
  60.0 0.1 pad_maximum_fusion
  60.1 67.9 %conditional.1 = (bf16[1,192,2048]{2,1,0:T(8,128)(2,1)S(1)}) conditional(s32[]{:T(128)} %bitcast.11, (pred[4,4]{1,0:T(4,128)(4,1)S(1)}, s32[4,4]{1,0:T(4,128)S(1)}, s32[4,4]{1,0:T(4,128)S(1)}, bf16[4,3,128]{2,1,0:T(4,128)(2,1)S(1)}, bf16[4,192,384]{2,1,0:T(8,128)(2,1)S(1)}, /*index=5*/s32[4,8,128]{2,1,0:T(8,128)S(1)}, f32[4,192,16]{2,1,0:T(8,128)S(1)}, ...), branch_computations={%region_3.5_spmd, %region_5.7_spmd} | conditional | flops 30000019456 | bytes 25187014 | solution.py:832
  60.3 0.1 select_reduce_fusion.1.order_ref
  60.4 41.8 %gather_kv.3.kv_ref = bf16[2,14,8,208,128]{4,3,2,1,0:T(8,128)(2,1)S(1)} custom-call(s32[4]{0:T(128)S(1)} %select_reduce_fusion.1.order_ref, bf16[4,192,384]{2,1,0:T(8,128)(2,1)S(1)} %get-tuple-element.99.got_ref.main_ref, bf16[4,16,128]{2,1,0:T(8,128)(2,1)S(1)} %pad.15.pairs_ref), custom_call_target="tpu_custom_call" | custom-call | flops 30000001024 | bytes 8388608 | tf_op jit(solution)/shard_map/cond/branch_1_fun/gather_kv/pallas_call | solution.py:525
  102.3 0.0 copy-start.2
  102.3 13.8 %attend.3.att_ref = bf16[4,192,256]{2,1,0:T(8,128)(2,1)S(1)} custom-call(s32[4]{0:T(128)S(1)} %select_reduce_fusion.1.order_ref, s32[4,8,128]{2,1,0:T(8,128)S(1)} %get-tuple-element.98.ints_ref, bf16[4,192,384]{2,1,0:T(8,128)(2,1)S(1)} %get-tuple-element.99.got_ref.main_ref, f32[4,192,16]{2,1,0:T(8,128)S(1)} %get-tuple-element.100.gate_ref, ...), custom_call_target="tpu_custom_call" | custom-call | tf_op jit(solution)/shard_map/cond/branch_1_fun/attend/pallas_call | solution.py:691
  116.1 0.0 copy-done.2
  116.1 11.9 %finish.5 = bf16[192,2048]{1,0:T(8,128)(2,1)S(1)} custom-call(s32[1]{0:T(128)} %get-tuple-element.94.len_ref, bf16[4,192,256]{2,1,0:T(8,128)(2,1)S(1)} %attend.3.att_ref, bf16[2,8,8,32,512]{4,3,2,1,0:T(8,128)(2,1)S(1)} %copy-done.2), custom_call_target="tpu_custom_call" | custom-call | tf_op jit(solution)/shard_map/cond/branch_1_fun/finish/pallas_call | solution.py:767
  128.1 0.9 copy.27
  (8 shorter events, 0.1 us)
Async XLA Ops:
  0.0 59.3 %copy-start = (bf16[4096,64]{0,1:T(8,128)(2,1)S(1)}, bf16[4096,64]{0,1:T(8,128)(2,1)}, u32[]{:S(2)}) copy-start(bf16[4096,64]{0,1:T(8,128)(2,1)} %param.19) | copy-start | bytes 1572868
  5.5 54.3 %copy-start.3 = (bf16[4096,64]{0,1:T(8,128)(2,1)S(1)}, bf16[4096,64]{0,1:T(8,128)(2,1)}, u32[]{:S(2)}) copy-start(bf16[4096,64]{0,1:T(8,128)(2,1)} %param.20) | copy-start | bytes 1572868
  102.3 13.8 %copy-start.2 = (bf16[2,8,8,32,512]{4,3,2,1,0:T(8,128)(2,1)S(1)}, bf16[2,8,8,32,512]{4,3,2,1,0:T(8,128)(2,1)}, u32[]{:S(2)}) copy-start(bf16[2,8,8,32,512]{4,3,2,1,0:T(8,128)(2,1)} %get-tuple-element.102.wo_ref) | copy-start | bytes 12582916 | tf_op jit(solution)/shard_map/cond

commit v5 on v4

--- a/solution.py
+++ b/solution.py
@@ -18,7 +18,7 @@
 N = 8
 ROWS = 208
 HALF = 192
-SPLIT = 112
+SPLIT = 96
 MASKED = -1e30
 VMEM = pltpu.MemorySpace.VMEM
 SMEM = pltpu.MemorySpace.SMEM

time: 129 us -> 127 us (0.984)
  Pallas kernels: 118 us -> 116 us
    pallas_call x1, Pallas kernels: 41.8 us -> 39.7 us  [gather_kv(): pl.pallas_call(functools.partial(kv_kernel, spans), out_shape=jax.ShapeDt...]
where the time goes in v5:
time: 127 us
  Pallas kernels  116 us (91%)
  local copies, waits for them, and re-layouts  4.7 us (4%)
  other arithmetic  2.78 us (2%)
  between operations  2.72 us (2%)
    pallas_call x1, Pallas kernels, entry(): pl.pallas_call(entry_kernel, out_shape=[jax.ShapeDtypeStruct((4, HALF, w....  50.4 us
    pallas_call x1, Pallas kernels, gather_kv(): pl.pallas_call(functools.partial(kv_kernel, spans), out_shape=jax.ShapeDt...  39.7 us
    pallas_call x1, Pallas kernels, attend(): pl.pallas_call(functools.partial(attend_kernel, spans), out_shape=jax.Sha...  13.8 us
    pallas_call x1, Pallas kernels, finish(): pl.pallas_call(finish_kernel, out_shape=jax.ShapeDtypeStruct((HALF, 2048)...  12.1 us

profile of v5, /device:TPU:1, one launch (start us, length us, event | category | flops | bytes accessed | tf_op | source)
XLA Modules:
  0.0 126.9 jit_solution(6368244593628485419)
XLA Ops:
  0.0 0.0 copy-start
  0.7 0.9 fusion.12
  1.6 0.1 copy.21
  1.7 0.1 broadcast_in_dim.50
  1.8 0.7 copy.22
  2.5 0.7 select_select_fusion.ints_ref
  3.2 0.9 fusion.17
  4.0 0.7 fusion.16
  4.8 0.7 maximum_select_fusion.w_ref
  5.5 0.0 copy-start.3
  5.5 50.4 %entry.1 = (bf16[4,192,384]{2,1,0:T(8,128)(2,1)S(1)}, f32[4,192,16]{2,1,0:T(8,128)S(1)}, bf16[2,8,8,32,512]{4,3,2,1,0:T(8,128)(2,1)}, s32[4,8,128]{2,1,0:T(8,128)S(1)}) custom-call(bf16[384,2048]{1,0:T(8,128)(2,1)} %bitcast.29, bf16[32,384]{1,0:T(8,128)(2,1)} %maximum_select_fusion.w_ref, bf16[32,512]{1,0:T(8,128)(2,1)} %bitcast.31, ...), custom_call_target="tpu_custom_call" | custom-call | flops 30000001024 | bytes 8388608 | tf_op jit(solution)/shard_map/entry/pallas_call | solution.py:442
  55.9 0.2 slice_reduce_fusion
  56.1 0.2 convert_reduce_fusion
  56.3 0.1 select_reduce_fusion.2
  56.4 0.7 fusion.19
  59.0 0.1 fusion.15
  59.1 0.2 dot_general.10
  59.3 0.0 copy-done
  59.3 0.3 convolution_convert_fusion.1
  59.6 0.2 dot_general.12
  59.7 0.0 copy-done.3
  59.8 0.3 convolution_convert_fusion
  60.0 0.1 pad_maximum_fusion
  60.1 65.9 %conditional.1 = (bf16[1,192,2048]{2,1,0:T(8,128)(2,1)S(1)}) conditional(s32[]{:T(128)} %bitcast.11, (pred[4,4]{1,0:T(4,128)(4,1)S(1)}, s32[4,4]{1,0:T(4,128)S(1)}, s32[4,4]{1,0:T(4,128)S(1)}, bf16[4,3,128]{2,1,0:T(4,128)(2,1)S(1)}, bf16[4,192,384]{2,1,0:T(8,128)(2,1)S(1)}, /*index=5*/s32[4,8,128]{2,1,0:T(8,128)S(1)}, f32[4,192,16]{2,1,0:T(8,128)S(1)}, ...), branch_computations={%region_3.5_spmd, %region_5.7_spmd} | conditional | flops 30000019456 | bytes 25187014 | solution.py:832
  60.3 0.1 select_reduce_fusion.1.order_ref
  60.4 39.7 %gather_kv.3.kv_ref = bf16[2,14,8,208,128]{4,3,2,1,0:T(8,128)(2,1)S(1)} custom-call(s32[4]{0:T(128)S(1)} %select_reduce_fusion.1.order_ref, bf16[4,192,384]{2,1,0:T(8,128)(2,1)S(1)} %get-tuple-element.99.got_ref.main_ref, bf16[4,16,128]{2,1,0:T(8,128)(2,1)S(1)} %pad.15.pairs_ref), custom_call_target="tpu_custom_call" | custom-call | flops 30000001024 | bytes 8388608 | tf_op jit(solution)/shard_map/cond/branch_1_fun/gather_kv/pallas_call | solution.py:525
  100.1 0.0 copy-start.2
  100.1 13.8 %attend.3.att_ref = bf16[4,192,256]{2,1,0:T(8,128)(2,1)S(1)} custom-call(s32[4]{0:T(128)S(1)} %select_reduce_fusion.1.order_ref, s32[4,8,128]{2,1,0:T(8,128)S(1)} %get-tuple-element.98.ints_ref, bf16[4,192,384]{2,1,0:T(8,128)(2,1)S(1)} %get-tuple-element.99.got_ref.main_ref, f32[4,192,16]{2,1,0:T(8,128)S(1)} %get-tuple-element.100.gate_ref, ...), custom_call_target="tpu_custom_call" | custom-call | tf_op jit(solution)/shard_map/cond/branch_1_fun/attend/pallas_call | solution.py:691
  113.9 0.0 copy-done.2
  114.0 12.1 %finish.5 = bf16[192,2048]{1,0:T(8,128)(2,1)S(1)} custom-call(s32[1]{0:T(128)} %get-tuple-element.94.len_ref, bf16[4,192,256]{2,1,0:T(8,128)(2,1)S(1)} %attend.3.att_ref, bf16[2,8,8,32,512]{4,3,2,1,0:T(8,128)(2,1)S(1)} %copy-done.2), custom_call_target="tpu_custom_call" | custom-call | tf_op jit(solution)/shard_map/cond/branch_1_fun/finish/pallas_call | solution.py:767
  126.0 0.9 copy.27
  (8 shorter events, 0.1 us)
Async XLA Ops:
  0.0 59.3 %copy-start = (bf16[4096,64]{0,1:T(8,128)(2,1)S(1)}, bf16[4096,64]{0,1:T(8,128)(2,1)}, u32[]{:S(2)}) copy-start(bf16[4096,64]{0,1:T(8,128)(2,1)} %param.19) | copy-start | bytes 1572868
  5.5 54.3 %copy-start.3 = (bf16[4096,64]{0,1:T(8,128)(2,1)S(1)}, bf16[4096,64]{0,1:T(8,128)(2,1)}, u32[]{:S(2)}) copy-start(bf16[4096,64]{0,1:T(8,128)(2,1)} %param.20) | copy-start | bytes 1572868
  100.1 13.8 %copy-start.2 = (bf16[2,8,8,32,512]{4,3,2,1,0:T(8,128)(2,1)S(1)}, bf16[2,8,8,32,512]{4,3,2,1,0:T(8,128)(2,1)}, u32[]{:S(2)}) copy-start(bf16[2,8,8,32,512]{4,3,2,1,0:T(8,128)(2,1)} %get-tuple-element.102.wo_ref) | copy-start | bytes 12582916 | tf_op jit(solution)/shard_map/cond
